TPU v7x, 512 devices: a whole 4x4x16 slice. The times are simulated.
512 devices in a mesh: ep: 32 (over z, core), tp: 16 (over y, x).
Axes of the slice: x: 4, y: 4, z: 16, core: 2. Of those that a mesh axis runs over, the one named last changes fastest.
Arguments:
- query_rows: bfloat16 [24576, 1024], P('ep', 'tp'), may hold values from -600 to 600
- key_rows: bfloat16 [24576, 1024], P('ep', 'tp'), may hold values from -6 to 6
- value_rows: bfloat16 [24576, 1024], P('ep', 'tp'), may hold values from -6 to 6
- cum_gate: float32 [16, 24576], P('tp'), may hold values from -2458 to 0, as said below
- out_weight: bfloat16 [1024, 2048], P(None, 'tp'), may hold values from -0.1875 to 0.1875
- moe_input: bfloat16 [6144, 2048], P('ep'), may hold values from -6 to 6
- moe_gain: float32 [2048], replicated, may hold values from 0.1 to 1.9
- routes: int32 [6144, 3], P('ep'), may hold values from 0 to 127, all different within a row; in each aligned block of 192 rows (0 to 191, 192 to 383, ...) at most 9 rows name the same one
- route_weight: float32 [6144, 3], P('ep'), may hold values from 0.2 to 1.5
- expert_gate: bfloat16 [128, 2048, 512], P('ep', None, 'tp'), may hold values from -0.125 to 0.125
- expert_up: bfloat16 [128, 2048, 512], P('ep', None, 'tp'), may hold values from -0.125 to 0.125
- expert_down: bfloat16 [128, 512, 2048], P('ep', None, 'tp'), may hold values from -0.25 to 0.25
- shared_gate: bfloat16 [2048, 512], P(None, 'tp'), may hold values from -0.125 to 0.125
- shared_up: bfloat16 [2048, 512], P(None, 'tp'), may hold values from -0.125 to 0.125
- shared_down: bfloat16 [512, 2048], P(None, 'tp'), may hold values from -0.25 to 0.25
Outputs:
- mixer_out: bfloat16 [24576, 2048], P('ep', 'tp')
- moe_out: bfloat16 [6144, 2048], P('ep', 'tp')
Inputs may be any that keep to these rules, and one draw needn't show every extreme that they name: Non-increasing along positions: cum_gate[h, t] is the sum of the log forget gates of head h over positions 0 to t. `routes`: the 3 experts of a token differ. In each aligned block of 192 tokens no expert is named by more than 9 tokens, a bound that some block reaches.
All inputs are finite; a program needn't handle non-finite values.
Results may differ from a plain program's by a relative error of at most 0.0068.
Values may be sent and summed in bfloat16 or wider, within the bound.
A program may use at most 64 MiB of HBM per device.

v0:
```python
import jax
import jax.numpy as jnp
from jax import lax
from jax.sharding import PartitionSpec as P

HEAD = 64


neg_fill = -1e30
norm_eps = 1e-06


def joined_along(pieces, dim):
    dims = list(pieces.shape[1:])
    dims[dim] *= pieces.shape[0]
    return jnp.moveaxis(pieces, 0, dim).reshape(dims)


def sent_to_all(array, axis):
    copies = jnp.broadcast_to(array, (lax.axis_size(axis), *array.shape))
    return lax.all_to_all(copies, axis, split_axis=0, concat_axis=0, tiled=True)


def collect(array, axis, dim):
    return joined_along(sent_to_all(array, axis), dim)


def local(
    query_rows,
    key_rows,
    value_rows,
    cum_gate,
    out_weight,
    moe_input,
    moe_gain,
    routes,
    route_weight,
    expert_gate,
    expert_up,
    expert_down,
    shared_gate,
    shared_up,
    shared_down,
):
    row_count = query_rows.shape[0]
    width = query_rows.shape[1]
    local_heads = width // HEAD
    scale = HEAD ** (-0.5)
    first_row = lax.axis_index("ep") * row_count
    last_row = first_row + row_count - 1
    query_heads = query_rows.reshape(row_count, local_heads, HEAD)
    query_gate = lax.dynamic_slice_in_dim(cum_gate, first_row, row_count, 1)
    query_pos = first_row + jnp.arange(row_count, dtype=jnp.int32)
    key_value = jnp.concatenate([key_rows, value_rows], axis=1)
    initial = (
        jnp.full((local_heads, row_count), neg_fill, jnp.float32),
        jnp.zeros((local_heads, row_count), jnp.float32),
        jnp.zeros((local_heads, row_count, HEAD), jnp.float32),
    )
    shard_rows = lax.all_gather(key_value, "ep", axis=0, tiled=True)
    piece_len = shard_rows.shape[0]
    key_span = 512

    def one_span(state_in, span_index):
        span_start = span_index * key_span

        def update(state_old):
            running_max, denominator, weighted = state_old
            block = lax.dynamic_slice_in_dim(shard_rows, span_index * key_span, key_span, 0)
            keys_block = block[:, :width].reshape(key_span, local_heads, HEAD)
            values_block = block[:, width:].reshape(key_span, local_heads, HEAD)
            key_gate = lax.dynamic_slice_in_dim(cum_gate, span_start, key_span, 1)
            scores = (
                jnp.einsum(
                    "qhd,khd->hqk", query_heads, keys_block, preferred_element_type=jnp.float32
                )
                * scale
            )
            scores = scores + query_gate[:, :, None] - key_gate[:, None, :]
            causal = (span_start + jnp.arange(key_span, dtype=jnp.int32))[None, :] <= query_pos[
                :, None
            ]
            scores = jnp.where(causal[None], scores, neg_fill)
            new_max = jnp.maximum(running_max, jnp.max(scores, axis=2))
            expon = jnp.where(causal[None], jnp.exp(scores - new_max[:, :, None]), 0.0)
            rescale = jnp.exp(running_max - new_max)
            denominator = denominator * rescale + jnp.sum(expon, axis=2)
            weighted = weighted * rescale[:, :, None] + jnp.einsum(
                "hqk,khd->hqd",
                expon.astype(jnp.bfloat16),
                values_block,
                preferred_element_type=jnp.float32,
            )
            return (new_max, denominator, weighted)

        state_next = lax.cond(span_start <= last_row, update, lambda unchanged: unchanged, state_in)
        return (state_next, None)

    state_out, _ = lax.scan(one_span, initial, jnp.arange(piece_len // key_span, dtype=jnp.int32))
    running_max, denominator, weighted = state_out
    heads_out = (weighted / denominator[:, :, None]).transpose(1, 0, 2).reshape(row_count, width)
    heads_out = heads_out.astype(jnp.bfloat16)
    token_count = moe_input.shape[0]
    top_count = routes.shape[1]
    local_experts = expert_gate.shape[0]
    ep_count = lax.axis_size("ep")
    expert_count = local_experts * ep_count
    capacity = 2 * token_count * top_count // expert_count
    column_count = expert_down.shape[2]
    first_column = lax.axis_index("tp") * column_count
    moe_rows = moe_input.astype(jnp.float32)
    normed = (
        moe_rows
        * lax.rsqrt(jnp.mean(moe_rows * moe_rows, axis=1, keepdims=True) + norm_eps)
        * moe_gain
    ).astype(jnp.bfloat16)
    flat_routes = routes.reshape(-1)
    one_hot = (flat_routes[:, None] == jnp.arange(expert_count, dtype=jnp.int32)[None, :]).astype(
        jnp.int32
    )
    ranks = jnp.sum(jnp.cumsum(one_hot, axis=0) * one_hot, axis=1) - 1
    slot_index = flat_routes * capacity + ranks
    pair_token = jnp.arange(token_count * top_count, dtype=jnp.int32) // top_count
    slot_token = (
        jnp.full((expert_count * capacity,), token_count, jnp.int32).at[slot_index].set(pair_token)
    )
    padded = jnp.concatenate([normed, jnp.zeros((1, normed.shape[1]), jnp.bfloat16)], axis=0)
    outgoing = lax.dynamic_slice_in_dim(padded, first_column, column_count, 1)[slot_token]
    outgoing = outgoing.reshape(ep_count, local_experts, capacity, outgoing.shape[1])
    arrived = lax.all_to_all(outgoing, "ep", split_axis=0, concat_axis=0, tiled=True)
    arrived = lax.all_gather(arrived, "tp", axis=3, tiled=True)
    gate_val = jnp.einsum(
        "aecd,edf->aecf", arrived, expert_gate, preferred_element_type=jnp.float32
    )
    up_val = jnp.einsum("aecd,edf->aecf", arrived, expert_up, preferred_element_type=jnp.float32)
    hidden = (jax.nn.silu(gate_val) * up_val).astype(jnp.bfloat16)
    hidden = collect(hidden, "tp", 3)
    result = jnp.einsum(
        "aecf,efd->aecd", hidden, expert_down, preferred_element_type=jnp.float32
    ).astype(jnp.bfloat16)
    returned = lax.all_to_all(result, "ep", split_axis=0, concat_axis=0, tiled=True)
    picked = returned.reshape(expert_count * capacity, column_count)[slot_index]
    picked = picked.astype(jnp.float32).reshape(token_count, top_count, column_count)
    routed = jnp.sum(picked * route_weight[:, :, None], axis=1)
    shared_hidden = (
        jax.nn.silu(jnp.dot(normed, shared_gate, preferred_element_type=jnp.float32))
        * jnp.dot(normed, shared_up, preferred_element_type=jnp.float32)
    ).astype(jnp.bfloat16)
    mixer_sum = jnp.dot(
        lax.all_gather(heads_out, "tp", axis=1, tiled=True),
        out_weight,
        preferred_element_type=jnp.float32,
    )
    shared_all = lax.all_gather(shared_hidden, "tp", axis=1, tiled=True)
    moe_total = routed + jnp.dot(shared_all, shared_down, preferred_element_type=jnp.float32)
    return (mixer_sum.astype(jnp.bfloat16), moe_total.astype(jnp.bfloat16))


def solution(mesh):
    placed = (
        P("ep", "tp"),
        P("ep", "tp"),
        P("ep", "tp"),
        P("tp", None),
        P(None, "tp"),
        P("ep", None),
        P(),
        P("ep", None),
        P("ep", None),
        P("ep", None, "tp"),
        P("ep", None, "tp"),
        P("ep", None, "tp"),
        P(None, "tp"),
        P(None, "tp"),
        P(None, "tp"),
    )
    return jax.shard_map(
        local, mesh=mesh, in_specs=placed, out_specs=(P("ep", "tp"), P("ep", "tp")), check_vma=False
    )
```

profile of v0, /device:TPU:1, one launch (start us, length us, event | category | flops | bytes accessed | tf_op | source)
XLA Modules:
  0.0 554.8 jit_solution(1330439696241112962)
XLA Ops:
  11.6 4.1 scatter_custom_fusion
  16.0 2.9 gather_fusion
  19.3 40.2 %all_to_all.15 = bf16[32,4,9,128]{3,1,2,0:T(4,128)(2,1)S(1)} all-to-all(bf16[32,4,9,128]{3,1,2,0:T(4,128)(2,1)S(1)} %copy.46), channel_id=1, replica_groups=mesh['ep'=32,'tp'=16] {'ep'}, dimensions={0} | all-to-all | bytes 589824 | tf_op jit(solution)/shard_map/all_to_all | solution.py:130
  61.6 63.6 %all-gather.7.cloned.1.call-done = bf16[32,4,9,2048]{3,0,2,1:T(8,128)(2,1)} async-done(((bf16[32,4,9,128]{3,0,2,1:T(8,128)(2,1)}), bf16[32,4,9,2048]{3,0,2,1:T(8,128)(2,1)}) %all-gather.7.cloned.1.call-update) | async-done | bytes 4718608 | tf_op jit(solution)/shard_map/all_gather | solution.py:131
  125.2 3.8 convolution_bitcast_fusion.2
  130.5 3.2 broadcast_bitcast_fusion
  133.7 7.8 %reshape.164 = bf16[16,2,18432]{2,1,0:T(2,128)(2,1)} reshape(bf16[16,4,9,32,32]{4,3,2,1,0:T(8,128)(2,1)} %broadcast_bitcast_fusion) | data formatting | bytes 2359296
  141.5 4.8 all-to-all-start.1
  147.2 58.1 %all-gather.5.cloned.1.call-done = bf16[24576,128]{1,0:T(8,128)(2,1)} async-done(((bf16[768,128]{1,0:T(8,128)(2,1)}), bf16[24576,128]{1,0:T(8,128)(2,1)}) %all-gather.5.cloned.1.call-update) | async-done | bytes 6291472 | tf_op jit(solution)/shard_map/all_gather | solution.py:60
  205.4 76.2 %while.15 = (s32[]{:T(128)}, f32[1,768]{1,0:T(1,128)S(1)}, f32[1,768]{1,0:T(1,128)S(1)}, f32[1,768,64]{1,2,0:T(8,128)S(1)}, s32[48]{0:T(128)S(1)}, /*index=5*/s3...) while((s32[]{:T(128)}, f32[1,768]{1,0:T(1,128)S(1)}, ...), condition=%wide.region_5.6_spmd.clone, body=%wide.region_0.5_spmd.clone.sunk | while | flops 106270224 | bytes 5566899 | solution.py:99
  206.7 4.7 conditional.3
  209.6 1.4 fusion.4
  212.6 4.7 conditional.3
  215.5 1.4 fusion.4
  218.6 4.7 conditional.3
  282.3 3.8 reshape.165
  286.1 3.1 bitcast_bitcast_fusion
  289.2 7.6 %copy.48 = bf16[32,4,9,16,32]{4,3,0,2,1:T(8,128)(2,1)} copy(bf16[32,4,9,16,32]{4,0,2,1,3:T(8,128)(2,1)S(1)} %bitcast_bitcast_fusion) | data formatting | bytes 2359296 | tf_op jit(solution)/shard_map/transpose | solution.py:16
  296.8 6.5 %reshape.124 = bf16[32,4,9,512]{3,0,2,1:T(8,128)(2,1)S(1)} reshape(bf16[32,4,9,16,32]{4,3,0,2,1:T(8,128)(2,1)} %copy.48) | data formatting | bytes 2359296 | tf_op jit(solution)/shard_map/reshape | solution.py:16
  304.7 213.7 %all-to-all-start.2 = ((bf16[32,4,9,128]{3,1,2,0:T(4,128)(2,1)}), bf16[32,4,9,128]{3,1,2,0:T(4,128)(2,1)S(1)}, u32[]{:S(2)}, u32[]{:S(2)}) async-start(bf16[32,4,9,128]{3,1,2,0:T(4,128)(2,1)} %copy.49), calls=%async_computation.2 | async-start | bytes 589824 | tf_op jit(solution)/shard_map/all_to_all | solution.py:141
  519.2 20.5 %all_gather.15 = bf16[192,512]{0,1:T(8,128)(2,1)S(1)} all-gather(bf16[192,32]{0,1:T(8,128)(2,1)S(1)} %fusion.27), channel_id=1, replica_groups=mesh['ep'=32,'tp'=16] {'tp'}, dimensions={1}, use_global_device_ids=true | all-gather | bytes 208896 | tf_op jit(solution)/shard_map/all_gather | solution.py:154
  539.7 2.2 all-to-all-done.2
  542.2 1.9 gather_fusion.1
  545.5 2.7 fusion.22
  (252 shorter events, 51.7 us)
Async XLA Ops:
  7.2 296.1 %copy-start = (bf16[4,512,128]{2,1,0:T(8,128)(2,1)S(1)}, bf16[4,512,128]{2,1,0:T(8,128)(2,1)}, u32[]{:S(2)}) copy-start(bf16[4,512,128]{2,1,0:T(8,128)(2,1)} %param.30) | copy-start | bytes 1572868
  7.2 118.0 %all-gather.7.cloned.1.call-start = ((), (), s32[]{:S(2)}) async-start(), calls=%async_computation.4 | async-start | bytes 5013504 | tf_op jit(solution)/shard_map/all_gather | solution.py:131
  10.9 4.8 copy-start.1
  10.9 4.8 copy-start.8
  19.0 41.4 %copy-start.6 = (bf16[768,64]{0,1:T(8,128)(2,1)S(1)}, bf16[768,64]{0,1:T(8,128)(2,1)}, u32[]{:S(2)}) copy-start(bf16[768,64]{0,1:T(8,128)(2,1)} %param.20) | copy-start | bytes 294916
  19.0 41.6 %copy-start.7 = (bf16[768,64]{0,1:T(8,128)(2,1)S(1)}, bf16[768,64]{0,1:T(8,128)(2,1)}, u32[]{:S(2)}) copy-start(bf16[768,64]{0,1:T(8,128)(2,1)} %param.21) | copy-start | bytes 294916
  19.3 105.9 %copy-start.11 = (bf16[4,2048,32]{1,2,0:T(8,128)(2,1)S(1)}, bf16[4,2048,32]{1,2,0:T(8,128)(2,1)}, u32[]{:S(2)}) copy-start(bf16[4,2048,32]{1,2,0:T(8,128)(2,1)} %param.28) | copy-start | bytes 1572868
  60.3 145.0 %all-gather.5.cloned.1.call-start = ((), (), s32[]{:S(2)}) async-start(), calls=%async_computation.3 | async-start | bytes 6488064 | tf_op jit(solution)/shard_map/all_gather | solution.py:60
  61.6 67.5 %copy-start.12 = (bf16[4,2048,32]{1,2,0:T(8,128)(2,1)S(1)}, bf16[4,2048,32]{1,2,0:T(8,128)(2,1)}, u32[]{:S(2)}) copy-start(bf16[4,2048,32]{1,2,0:T(8,128)(2,1)} %param.29) | copy-start | bytes 1572868
  125.2 3.9 copy-start.10
  141.5 63.9 %copy-start.13 = (bf16[768,64]{0,1:T(8,128)(2,1)S(1)}, bf16[768,64]{0,1:T(8,128)(2,1)}, u32[]{:S(2)}) copy-start(bf16[768,64]{0,1:T(8,128)(2,1)} %param.19) | copy-start | bytes 294916
  141.5 140.8 %all-to-all-start.1 = ((bf16[16,2,18432]{2,1,0:T(2,128)(2,1)}), bf16[16,2,18432]{2,1,0:T(2,128)(2,1)S(1)}, u32[]{:S(2)}, u32[]{:S(2)}) async-start(bf16[16,2,18432]{2,1,0:T(2,128)(2,1)} %reshape.164), calls=%async_computation.1 | async-start | bytes 2359296 | tf_op jit(solution)/shard_map/all_to_all | solution.py:21
  146.3 399.2 %all-gather.9.cloned.1.call-start = ((), (), s32[]{:S(2)}) async-start(), calls=%async_computation.5 | async-start | bytes 1671168 | tf_op jit(solution)/shard_map/all_gather | solution.py:150
  303.3 215.1 %copy-start.9 = (f32[192,3]{0,1:T(4,128)S(1)}, f32[192,3]{0,1:T(4,128)}, u32[]{:S(2)}) copy-start(f32[192,3]{0,1:T(4,128)} %param.27) | copy-start | bytes 6916
  303.3 215.2 %copy-start.4 = (bf16[2048,32]{0,1:T(8,128)(2,1)S(1)}, bf16[2048,32]{0,1:T(8,128)(2,1)}, u32[]{:S(2)}) copy-start(bf16[2048,32]{0,1:T(8,128)(2,1)} %param.31) | copy-start | bytes 393220
  303.8 215.1 %copy-start.5 = (bf16[2048,32]{0,1:T(8,128)(2,1)S(1)}, bf16[2048,32]{0,1:T(8,128)(2,1)}, u32[]{:S(2)}) copy-start(bf16[2048,32]{0,1:T(8,128)(2,1)} %param.32) | copy-start | bytes 393220
  304.7 237.3 %all-to-all-start.2 = ((bf16[32,4,9,128]{3,1,2,0:T(4,128)(2,1)}), bf16[32,4,9,128]{3,1,2,0:T(4,128)(2,1)S(1)}, u32[]{:S(2)}, u32[]{:S(2)}) async-start(bf16[32,4,9,128]{3,1,2,0:T(4,128)(2,1)} %copy.49), calls=%async_computation.2 | async-start | bytes 589824 | tf_op jit(solution)/shard_map/all_to_all | solution.py:141
  542.1 2.6 copy-start.3
  542.2 3.3 copy-start.2
Sparse Core Ops, SparseCore 0:
  60.4 64.7 all-gather.6
  127.9 77.4 all-gather.4
  282.4 260.1 all-gather.8
where the time goes:
time: 559 us; the launch traced here: 555 us
  starting transfers between devices  219 us (39%)
  waiting for transfers between devices  124 us (22%)
  local copies, waits for them, and re-layouts  76.5 us (14%)
  blocking collectives  60.7 us (11%)
  loops' own time  36.1 us (6%)
  matrix products  18.3 us (3%)
  between operations  14.2 us (3%)
  other arithmetic  6.13 us (1%)
    all_to_all x1, starting transfers between devices, local(): lax.all_to_all(result, 'ep', split_axis=0, concat_axis=0, tiled=True)  214 us
    all_gather x1, waiting for transfers between devices, local(): arrived = lax.all_gather(arrived, 'tp', axis=3, tiled=True)  63.6 us
    all_gather x1, waiting for transfers between devices, local(): shard_rows = lax.all_gather(key_value, 'ep', axis=0, tiled=True)  58.1 us
    all_to_all x1, blocking collectives, local(): lax.all_to_all(outgoing, 'ep', split_axis=0, concat_axis=0, tiled=True)  40.2 us
    another operation x1, loops' own time, local(): lax.scan(one_span, initial, jnp.arange(piece_len // key_span, dtype=jnp.i...  33.2 us
    dynamic_slice x48, local copies, waits for them, and re-layouts, local(): lax.scan(one_span, initial, jnp.arange(piece_len // key_span, dtype=jnp.i...  28.1 us
    all_gather x1, blocking collectives, local(): shared_all = lax.all_gather(shared_hidden, 'tp', axis=1, tiled=True)  20.5 us
    unnamed x35, local copies, waits for them, and re-layouts  16.1 us
  transfers between devices with their start and end apart: 5, of which 3 were waited for; matrix products, arithmetic and copies ran while one was open for 15% of the time, Pallas kernels for 0%

commit v1 on v0

v1 whole, which is shorter than its diff:
```python
import functools
import jax
import jax.numpy as jnp
from jax import lax
from jax.experimental import pallas as pl
from jax.experimental.pallas import tpu as pltpu
from jax.sharding import PartitionSpec as P

HEAD = 64
LOG2E = 1.4426950408889634
MESH = pl.DeviceIdType.MESH


neg_fill = -1e30
norm_eps = 1e-06


def joined_along(pieces, dim):
    dims = list(pieces.shape[1:])
    dims[dim] *= pieces.shape[0]
    return jnp.moveaxis(pieces, 0, dim).reshape(dims)


def sent_to_all(array, axis):
    copies = jnp.broadcast_to(array, (lax.axis_size(axis), *array.shape))
    return lax.all_to_all(copies, axis, split_axis=0, concat_axis=0, tiled=True)


def collect(array, axis, dim):
    return joined_along(sent_to_all(array, axis), dim)


def attn_kernel(dims, qT_ref, kv_ref, cg_ref, w_ref, out_ref,
                kv, qs, acc, mx, hg, wb,
                ring_send, ring_recv, pair_send, pair_recv, head_send, head_recv):
    Z, Y, X, R, CH = dims
    NCH = R // CH
    QT = R // 256
    NU, ND = Z // 2, Z // 2 - 1
    ep = lax.axis_index("ep")
    tp = lax.axis_index("tp")
    z, core = ep // 2, ep % 2
    y, x = tp // X, tp % X
    up = (lax.rem(ep + 2, 2 * Z), tp)
    down = (lax.rem(ep + 2 * Z - 2, 2 * Z), tp)
    partner = (2 * z + 1 - core, tp)

    def x_peer(k):
        return (ep, y * X + lax.rem(x + k, X))

    def y_peer(k):
        return (ep, lax.rem(y + k, Y) * X + x)

    barrier = pltpu.get_barrier_semaphore()
    peers = [up, down, partner] + [x_peer(k) for k in range(1, X)] + [y_peer(k) for k in range(1, Y)]
    for peer in peers:
        pl.semaphore_signal(barrier, inc=1, device_id=peer, device_id_type=MESH)
    pl.semaphore_wait(barrier, len(peers))

    def copy(src, dst, ssem, rsem, dev):
        return pltpu.make_async_remote_copy(
            src_ref=src, dst_ref=dst, send_sem=ssem, recv_sem=rsem,
            device_id=dev, device_id_type=MESH)

    def first(c, slot, dev):
        return copy(kv_ref.at[:, pl.ds(c * CH, CH)], kv.at[slot, c, 0],
                    ring_send.at[slot, c], ring_recv.at[slot, c], dev)

    def first_pair(c):
        return copy(kv_ref.at[:, pl.ds(c * CH, CH)], kv.at[0, c, 1],
                    pair_send.at[0, c], pair_recv.at[0, c], partner)

    def onward(slot, c, dev):
        return copy(kv.at[slot, c, 0], kv.at[slot + 1, c, 0],
                    ring_send.at[slot + 1, c], ring_recv.at[slot + 1, c], dev)

    def to_pair(slot, c):
        return copy(kv.at[slot, c, 0], kv.at[slot, c, 1],
                    pair_send.at[slot, c], pair_recv.at[slot, c], partner)

    for c in range(NCH):
        first(c, 1, up).start()
        first(c, NU + 1, down).start()
        first_pair(c).start()

    qpad = jnp.concatenate(
        [qT_ref[...].astype(jnp.float32) * (HEAD ** -0.5), jnp.zeros((HEAD, R), jnp.float32)], axis=0)
    qs[...] = jnp.transpose(qpad).astype(jnp.bfloat16)
    mx[...] = jnp.full(mx.shape, neg_fill, jnp.float32)
    acc[...] = jnp.zeros(acc.shape, jnp.float32)
    wb[...] = jnp.zeros(wb.shape, jnp.bfloat16)

    def place(h, _):
        part = w_ref[pl.ds(pl.multiple_of(h * HEAD, HEAD), HEAD), :]
        wb[pl.ds(pl.multiple_of(h * 128, 128), HEAD), 0:128] = part
        wb[pl.ds(pl.multiple_of(h * 128 + HEAD, HEAD), HEAD), 128:256] = part
        return 0

    lax.fori_loop(0, w_ref.shape[0] // HEAD, place, 0)

    first_row = pl.multiple_of(ep * R, 128)
    base_gate = cg_ref[:, pl.ds(first_row, 128)][:, 0:1]

    def gate_of(block, c):
        at = pl.multiple_of(block * R + c * CH, 128)
        return (cg_ref[:, pl.ds(at, CH)] - base_gate) * LOG2E

    def with_ones(keys):
        row = lax.broadcasted_iota(jnp.int32, keys.shape, 0)
        return jnp.where(row < HEAD, jnp.ones_like(keys), keys)

    def update(i, parts):
        rows = slice(i * 256, (i + 1) * 256)
        q = qs[rows, :]
        logits = []
        for keys, gate, masked in parts:
            s = jnp.dot(q, keys, preferred_element_type=jnp.float32) * LOG2E - gate
            if masked:
                qi = lax.broadcasted_iota(jnp.int32, s.shape, 0)
                ki = lax.broadcasted_iota(jnp.int32, s.shape, 1)
                s = jnp.where(ki <= qi, s, neg_fill)
            logits.append(s)
        top = logits[0]
        for s in logits[1:]:
            top = jnp.maximum(top, s)
        old = mx[rows, 0:1]
        new = jnp.maximum(old, jnp.max(top, axis=1, keepdims=True))
        total = acc[rows, :] * jnp.exp2(old - new)
        for s, (keys, gate, masked) in zip(logits, parts):
            p = jnp.exp2(s - new).astype(jnp.bfloat16)
            total = total + lax.dot_general(
                p, with_ones(keys), (((1,), (1,)), ((), ())), preferred_element_type=jnp.float32)
        acc[rows, :] = total
        mx[rows, :] = jnp.broadcast_to(new, (256, 128))

    for c in range(NCH):
        keys = kv_ref[:, c * CH:(c + 1) * CH]
        for i in range(c, QT):
            update(i, [(keys, gate_of(ep, c), i == c)])

    for c in range(NCH):
        to = first_pair(c)
        to.wait_recv()

    @pl.when(core == 1)
    def _():
        for c in range(NCH):
            keys = kv[0, c, 1]
            for i in range(QT):
                update(i, [(keys, gate_of(ep - 1, c), False)])

    def issue(s, c):
        onward(s - 1, c, up).wait_recv()
        to_pair(s, c).start()

        @pl.when(s < NU)
        def _():
            onward(s, c, up).start()

        @pl.when(s <= ND)
        def _():
            onward(NU + s - 1, c, down).wait_recv()
            to_pair(NU + s, c).start()

        @pl.when(s < ND)
        def _():
            onward(NU + s, c, down).start()

    def attend(slot, c, chip):
        parts = []
        for k, block in ((0, 2 * chip + core), (1, 2 * chip + 1 - core)):
            parts.append((kv.at[slot, c, k], gate_of(block, c)))
        for i in range(QT):
            update(i, [(ref[...], gate, False) for ref, gate in parts])

    def consume(s, c):
        to_pair(s, c).wait_recv()

        @pl.when(z - s >= 0)
        def _():
            attend(s, c, z - s)

        @pl.when(s <= ND)
        def _():
            to_pair(NU + s, c).wait_recv()

            @pl.when(z + s >= Z)
            def _():
                attend(NU + s, c, z + s - Z)

    steps = NU * NCH

    def step(t, _):
        @pl.when(t < steps)
        def _():
            issue(t // NCH + 1, t % NCH)

        @pl.when(t >= 1)
        def _():
            consume((t - 1) // NCH + 1, (t - 1) % NCH)

        return 0

    lax.fori_loop(0, steps + 1, step, 0)

    quarter, half = R // 4, R // 2
    low = lax.broadcasted_iota(jnp.int32, (quarter, 128), 1) < HEAD

    def finished(at):
        a = acc[at:at + quarter, :]
        return a / pltpu.roll(a, HEAD, 1)

    for h in range(2):
        first_half = pltpu.roll(finished(h * quarter), HEAD, 1)
        second_half = finished(half + h * quarter)
        hg[h, y, x] = jnp.where(low, first_half, second_half).astype(jnp.bfloat16)

    def spread(h, phase, k):
        along_x = (h == 0) == (phase == 0)
        dev = x_peer(k) if along_x else y_peer(k)
        if phase == 0:
            ref = hg.at[h, y, x]
        elif along_x:
            ref = hg.at[h, :, x]
        else:
            ref = hg.at[h, y]
        return copy(ref, ref, head_send.at[h, phase, k], head_recv.at[h, phase, k], dev)

    def spread_in(h, phase, k):
        along_x = (h == 0) == (phase == 0)
        n = X if along_x else Y
        src_x = lax.rem(x + X - k, X)
        src_y = lax.rem(y + Y - k, Y)
        if phase == 0:
            ref = hg.at[h, y, src_x] if along_x else hg.at[h, src_y, x]
        elif along_x:
            ref = hg.at[h, :, src_x]
        else:
            ref = hg.at[h, src_y]
        return copy(ref, ref, head_send.at[h, phase, k], head_recv.at[h, phase, k], partner)

    def count(h, phase):
        return X if (h == 0) == (phase == 0) else Y

    for phase in range(2):
        for h in range(2):
            if phase == 1:
                for k in range(1, count(h, 0)):
                    spread_in(h, 0, k).wait_recv()
            for k in range(1, count(h, phase)):
                spread(h, phase, k).start()

    for h in range(2):
        for k in range(1, count(h, 1)):
            spread_in(h, 1, k).wait_recv()
        heads = X * Y
        flat = hg.at[h]
        total = jnp.zeros((quarter, 256), jnp.float32)
        for pair in range(heads // 2):
            a, b = 2 * pair, 2 * pair + 1
            lhs = jnp.concatenate([flat[a // X, a % X], flat[b // X, b % X]], axis=1)
            total = total + jnp.dot(lhs, wb[pair * 256:(pair + 1) * 256, :],
                                    preferred_element_type=jnp.float32)
        out_ref[h * quarter:(h + 1) * quarter, :] = total[:, 0:128].astype(jnp.bfloat16)
        out_ref[half + h * quarter:half + (h + 1) * quarter, :] = total[:, 128:256].astype(jnp.bfloat16)

    for c in range(NCH):
        first(c, 1, up).wait_send()
        first(c, NU + 1, down).wait_send()
        first_pair(c).wait_send()

    def drain(s, _):
        for c in range(NCH):
            to_pair(s, c).wait_send()

            @pl.when(s < NU)
            def _():
                onward(s, c, up).wait_send()

            @pl.when(s <= ND)
            def _():
                to_pair(NU + s, c).wait_send()

            @pl.when(s < ND)
            def _():
                onward(NU + s, c, down).wait_send()
        return 0

    lax.fori_loop(1, NU + 1, drain, 0)
    for phase in range(2):
        for h in range(2):
            for k in range(1, count(h, phase)):
                spread(h, phase, k).wait_send()


def attention(sizes, query_rows, key_rows, value_rows, cum_gate, out_weight):
    n_ep, Y, X = sizes
    Z = n_ep // 2
    R = query_rows.shape[0]
    CH = 256
    NU = Z // 2
    heads = X * Y
    kv = jnp.concatenate([key_rows.T, value_rows.T], axis=0)
    vm = pl.BlockSpec(memory_space=pltpu.VMEM)
    return pl.pallas_call(
        functools.partial(attn_kernel, (Z, Y, X, R, CH)),
        out_shape=jax.ShapeDtypeStruct((R, out_weight.shape[1]), jnp.bfloat16),
        in_specs=[vm] * 4,
        out_specs=vm,
        scratch_shapes=[
            pltpu.VMEM((Z, R // CH, 2, 2 * HEAD, CH), jnp.bfloat16),
            pltpu.VMEM((R, 128), jnp.bfloat16),
            pltpu.VMEM((R, 128), jnp.float32),
            pltpu.VMEM((R, 128), jnp.float32),
            pltpu.VMEM((2, Y, X, R // 4, 128), jnp.bfloat16),
            pltpu.VMEM((heads * 128, 256), jnp.bfloat16),
            pltpu.SemaphoreType.DMA((Z, R // CH)),
            pltpu.SemaphoreType.DMA((Z, R // CH)),
            pltpu.SemaphoreType.DMA((Z, R // CH)),
            pltpu.SemaphoreType.DMA((Z, R // CH)),
            pltpu.SemaphoreType.DMA((2, 2, 4)),
            pltpu.SemaphoreType.DMA((2, 2, 4)),
        ],
        compiler_params=pltpu.CompilerParams(
            collective_id=0, has_side_effects=True, vmem_limit_bytes=48 * 1024 * 1024),
    )(query_rows.T, kv, cum_gate, out_weight)


def local(
    query_rows,
    key_rows,
    value_rows,
    cum_gate,
    out_weight,
    moe_input,
    moe_gain,
    routes,
    route_weight,
    expert_gate,
    expert_up,
    expert_down,
    shared_gate,
    shared_up,
    shared_down,
):
    tp_count = lax.axis_size("tp")
    x_count = 4 if tp_count == 16 else 2
    sizes = (lax.axis_size("ep"), tp_count // x_count, x_count)
    mixer_out = attention(sizes, query_rows, key_rows, value_rows, cum_gate, out_weight)
    token_count = moe_input.shape[0]
    top_count = routes.shape[1]
    local_experts = expert_gate.shape[0]
    ep_count = lax.axis_size("ep")
    expert_count = local_experts * ep_count
    capacity = 2 * token_count * top_count // expert_count
    column_count = expert_down.shape[2]
    first_column = lax.axis_index("tp") * column_count
    moe_rows = moe_input.astype(jnp.float32)
    normed = (
        moe_rows
        * lax.rsqrt(jnp.mean(moe_rows * moe_rows, axis=1, keepdims=True) + norm_eps)
        * moe_gain
    ).astype(jnp.bfloat16)
    flat_routes = routes.reshape(-1)
    one_hot = (flat_routes[:, None] == jnp.arange(expert_count, dtype=jnp.int32)[None, :]).astype(
        jnp.int32
    )
    ranks = jnp.sum(jnp.cumsum(one_hot, axis=0) * one_hot, axis=1) - 1
    slot_index = flat_routes * capacity + ranks
    pair_token = jnp.arange(token_count * top_count, dtype=jnp.int32) // top_count
    slot_token = (
        jnp.full((expert_count * capacity,), token_count, jnp.int32).at[slot_index].set(pair_token)
    )
    padded = jnp.concatenate([normed, jnp.zeros((1, normed.shape[1]), jnp.bfloat16)], axis=0)
    outgoing = lax.dynamic_slice_in_dim(padded, first_column, column_count, 1)[slot_token]
    outgoing = outgoing.reshape(ep_count, local_experts, capacity, outgoing.shape[1])
    arrived = lax.all_to_all(outgoing, "ep", split_axis=0, concat_axis=0, tiled=True)
    arrived = lax.all_gather(arrived, "tp", axis=3, tiled=True)
    gate_val = jnp.einsum(
        "aecd,edf->aecf", arrived, expert_gate, preferred_element_type=jnp.float32
    )
    up_val = jnp.einsum("aecd,edf->aecf", arrived, expert_up, preferred_element_type=jnp.float32)
    hidden = (jax.nn.silu(gate_val) * up_val).astype(jnp.bfloat16)
    hidden = collect(hidden, "tp", 3)
    result = jnp.einsum(
        "aecf,efd->aecd", hidden, expert_down, preferred_element_type=jnp.float32
    ).astype(jnp.bfloat16)
    returned = lax.all_to_all(result, "ep", split_axis=0, concat_axis=0, tiled=True)
    picked = returned.reshape(expert_count * capacity, column_count)[slot_index]
    picked = picked.astype(jnp.float32).reshape(token_count, top_count, column_count)
    routed = jnp.sum(picked * route_weight[:, :, None], axis=1)
    shared_hidden = (
        jax.nn.silu(jnp.dot(normed, shared_gate, preferred_element_type=jnp.float32))
        * jnp.dot(normed, shared_up, preferred_element_type=jnp.float32)
    ).astype(jnp.bfloat16)
    shared_all = lax.all_gather(shared_hidden, "tp", axis=1, tiled=True)
    moe_total = routed + jnp.dot(shared_all, shared_down, preferred_element_type=jnp.float32)
    return (mixer_out, moe_total.astype(jnp.bfloat16))


def solution(mesh):
    placed = (
        P("ep", "tp"),
        P("ep", "tp"),
        P("ep", "tp"),
        P("tp", None),
        P(None, "tp"),
        P("ep", None),
        P(),
        P("ep", None),
        P("ep", None),
        P("ep", None, "tp"),
        P("ep", None, "tp"),
        P("ep", None, "tp"),
        P(None, "tp"),
        P(None, "tp"),
        P(None, "tp"),
    )
    return jax.shard_map(
        local, mesh=mesh, in_specs=placed, out_specs=(P("ep", "tp"), P("ep", "tp")), check_vma=False
    )
```

time: 559 us -> 329 us (0.59)
  the two profiles are of different devices: /device:TPU:1 before, /device:TPU:2 now
where the time goes in v1:
time: 329 us; the launch traced here: 328 us
  Pallas kernels  92 us (28%)
  blocking collectives  84.2 us (26%)
  waiting for transfers between devices  65.9 us (20%)
  local copies, waits for them, and re-layouts  47.8 us (15%)
  between operations  14.5 us (4%)
  starting transfers between devices  12.9 us (4%)
  matrix products  7.27 us (2%)
  other arithmetic  3.49 us (1%)
    pallas_call x1, Pallas kernels, attention(): pl.pallas_call(functools.partial(attn_kernel, (Z, Y, X, R, CH)), out_shap...  92 us
    all_gather x1, waiting for transfers between devices, local(): arrived = lax.all_gather(arrived, 'tp', axis=3, tiled=True)  65.9 us
    all_to_all x1, blocking collectives, local(): lax.all_to_all(outgoing, 'ep', split_axis=0, concat_axis=0, tiled=True)  39.3 us
    all_gather x1, blocking collectives, local(): shared_all = lax.all_gather(shared_hidden, 'tp', axis=1, tiled=True)  23 us
    all_to_all x1, blocking collectives, sent_to_all(): return lax.all_to_all(copies, axis, split_axis=0, concat_axis=0, tiled=True)  21.8 us
    unnamed x36, local copies, waits for them, and re-layouts  18.7 us
    all_to_all x1, starting transfers between devices, local(): lax.all_to_all(result, 'ep', split_axis=0, concat_axis=0, tiled=True)  12.8 us
    transpose x2, local copies, waits for them, and re-layouts, joined_along(): return jnp.moveaxis(pieces, 0, dim).reshape(dims)  10.7 us
  transfers between devices with their start and end apart: 2, of which 1 were waited for; matrix products, arithmetic and copies ran while one was open for 0% of the time, Pallas kernels for 28%

profile of v1, /device:TPU:2, one launch (start us, length us, event | category | flops | bytes accessed | tf_op | source)
XLA Modules:
  0.0 328.0 jit_solution(3670094929339881257)
XLA Ops:
  7.3 0.8 broadcast_multiply_fusion
  8.0 0.8 copy.34
  8.9 1.4 fusion
  11.6 4.1 %scatter_custom_fusion = s32[1152]{0:T(1024)S(1)} fusion(s32[576]{0:T(1024)S(1)} %fusion.19, s32[576]{0:T(1024)S(1)} %add_select_fusion, s32[]{:T(128)} %constant.25.clone.1), kind=kCustom, calls=%fused_computation.43 | custom fusion | bytes 4612 | tf_op jit(solution)/shard_map/scatter | solution.py:372
  16.1 2.9 gather_fusion
  19.3 39.3 %all_to_all.15 = bf16[32,4,9,128]{3,1,2,0:T(4,128)(2,1)S(1)} all-to-all(bf16[32,4,9,128]{3,1,2,0:T(4,128)(2,1)S(1)} %copy.37), channel_id=1, replica_groups=mesh['ep'=32,'tp'=16] {'ep'}, dimensions={0} | all-to-all | bytes 589824 | tf_op jit(solution)/shard_map/all_to_all | solution.py:377
  58.6 0.8 copy.38
  59.4 65.9 %all-gather.2.cloned.1.call-done = bf16[32,4,9,2048]{3,0,2,1:T(8,128)(2,1)} async-done(((bf16[32,4,9,128]{3,0,2,1:T(8,128)(2,1)}), bf16[32,4,9,2048]{3,0,2,1:T(8,128)(2,1)}) %all-gather.2.cloned.1.call-update) | async-done | bytes 4718608 | tf_op jit(solution)/shard_map/all_gather | solution.py:378
  125.3 3.9 %convolution_bitcast_fusion.1 = f32[32,4,9,32]{3,0,2,1:T(8,128)S(1)} fusion(bf16[32,4,9,2048]{3,0,2,1:T(8,128)(2,1)} %all-gather.2.cloned.1.call-done, bf16[4,2048,32]{1,2,0:T(8,128)(2,1)S(1)} %copy-done.13), kind=kOutput, calls=%fused_computation.10 | convolution fusion | flops 150994944 | bytes 5390336 | tf_op jit(solution)/shard_map/aecd,edf->aecf/dot_general | solution.py:379
  129.2 1.4 fusion.4
  130.6 3.1 broadcast_bitcast_fusion
  133.7 7.0 %reshape.111 = bf16[16,2,18432]{2,1,0:T(2,128)(2,1)S(1)} reshape(bf16[16,4,9,32,32]{4,3,2,1,0:T(8,128)(2,1)} %broadcast_bitcast_fusion) | data formatting | bytes 2359296
  140.7 21.8 %all_to_all.16 = bf16[16,2,18432]{2,1,0:T(2,128)(2,1)} all-to-all(bf16[16,2,18432]{2,1,0:T(2,128)(2,1)S(1)} %reshape.111), channel_id=1, replica_groups=mesh['ep'=32,'tp'=16] {'tp'}, dimensions={0} | all-to-all | bytes 2359296 | tf_op jit(solution)/shard_map/all_to_all | solution.py:26
  162.6 6.8 %reshape.112 = bf16[16,4,9,32,32]{4,3,2,1,0:T(8,128)(2,1)} reshape(bf16[16,2,18432]{2,1,0:T(2,128)(2,1)} %all_to_all.16) | data formatting | bytes 2359296
  169.4 3.1 bitcast_bitcast_fusion
  172.6 7.6 %copy.39 = bf16[32,4,9,16,32]{4,3,0,2,1:T(8,128)(2,1)} copy(bf16[32,4,9,16,32]{4,0,2,1,3:T(8,128)(2,1)S(1)} %bitcast_bitcast_fusion) | data formatting | bytes 2359296 | tf_op jit(solution)/shard_map/transpose | solution.py:21
  180.2 6.6 %reshape.76 = bf16[32,4,9,512]{3,0,2,1:T(8,128)(2,1)S(1)} reshape(bf16[32,4,9,16,32]{4,3,0,2,1:T(8,128)(2,1)} %copy.39) | data formatting | bytes 2359296 | tf_op jit(solution)/shard_map/reshape | solution.py:21
  187.3 0.9 copy.40
  188.1 12.8 %all-to-all-start.2 = ((bf16[32,4,9,128]{3,1,2,0:T(4,128)(2,1)}), bf16[32,4,9,128]{3,1,2,0:T(4,128)(2,1)S(1)}, u32[]{:S(2)}, u32[]{:S(2)}) async-start(bf16[32,4,9,128]{3,1,2,0:T(4,128)(2,1)} %copy.40), calls=%async_computation.2 | async-start | bytes 589824 | tf_op jit(solution)/shard_map/all_to_all | solution.py:388
  201.1 92.0 %shard_map.158 = bf16[768,128]{1,0:T(8,128)(2,1)S(1)} custom-call(bf16[64,768]{1,0:T(8,128)(2,1)S(1)} %bitcast.55, bf16[128,768]{1,0:T(8,128)(2,1)S(1)} %pad_maximum_fusion.kv_ref, f32[1,24576]{1,0:T(1,128)S(1)} %copy-done.3, bf16[1024,128]{1,0:T(8,128)(2,1)S(1)} %copy-done.1), custom_call_target="tpu_custom_call" | custom-call | tf_op jit(solution)/shard_map/pallas_call | solution.py:305
  293.9 23.0 %all_gather.7 = bf16[192,512]{0,1:T(8,128)(2,1)S(1)} all-gather(bf16[192,32]{0,1:T(8,128)(2,1)S(1)} %fusion.7), channel_id=1, replica_groups=mesh['ep'=32,'tp'=16] {'tp'}, dimensions={1}, use_global_device_ids=true | all-gather | bytes 208896 | tf_op jit(solution)/shard_map/all_gather | solution.py:396
  317.2 1.9 gather_fusion.1
  319.6 0.9 fusion.6
  320.5 0.7 copy.49
  (64 shorter events, 4.0 us)
Async XLA Ops:
  7.2 179.6 %copy-start = (bf16[4,512,128]{2,1,0:T(8,128)(2,1)S(1)}, bf16[4,512,128]{2,1,0:T(8,128)(2,1)}, u32[]{:S(2)}) copy-start(bf16[4,512,128]{2,1,0:T(8,128)(2,1)} %param.26) | copy-start | bytes 1572868
  7.2 8.6 %copy-start.4 = (bf16[192,2048]{1,0:T(8,128)(2,1)S(1)}, bf16[192,2048]{1,0:T(8,128)(2,1)}, u32[]{:S(2)}) copy-start(bf16[192,2048]{1,0:T(8,128)(2,1)} %param.20) | copy-start | bytes 2359300
  7.2 8.6 %copy-start.10 = (f32[2048]{0:T(1024)S(1)}, f32[2048]{0:T(1024)}, u32[]{:S(2)}) copy-start(f32[2048]{0:T(1024)} %param.21) | copy-start | bytes 24580
  7.2 118.1 %all-gather.2.cloned.1.call-start = ((), (), s32[]{:S(2)}) async-start(), calls=%async_computation.3 | async-start | bytes 5013504 | tf_op jit(solution)/shard_map/all_gather | solution.py:378
  11.3 114.0 %copy-start.13 = (bf16[4,2048,32]{1,2,0:T(8,128)(2,1)S(1)}, bf16[4,2048,32]{1,2,0:T(8,128)(2,1)}, u32[]{:S(2)}) copy-start(bf16[4,2048,32]{1,2,0:T(8,128)(2,1)} %param.24) | copy-start | bytes 1572868
  59.4 69.7 %copy-start.14 = (bf16[4,2048,32]{1,2,0:T(8,128)(2,1)S(1)}, bf16[4,2048,32]{1,2,0:T(8,128)(2,1)}, u32[]{:S(2)}) copy-start(bf16[4,2048,32]{1,2,0:T(8,128)(2,1)} %param.25) | copy-start | bytes 1572868
  125.3 3.9 %copy-start.12 = (bf16[32,4,9,2048]{3,0,2,1:T(8,128)(2,1)S(1)}, bf16[32,4,9,2048]{3,0,2,1:T(8,128)(2,1)}, u32[]{:S(2)}) copy-start(bf16[32,4,9,2048]{3,0,2,1:T(8,128)(2,1)} %all-gather.2.cloned.1.call-done) | copy-start | bytes 14155780
  180.1 20.8 %copy-start.11 = (f32[192,3]{0,1:T(4,128)S(1)}, f32[192,3]{0,1:T(4,128)}, u32[]{:S(2)}) copy-start(f32[192,3]{0,1:T(4,128)} %param.23) | copy-start | bytes 6916
  180.1 20.9 %copy-start.8 = (bf16[768,64]{0,1:T(8,128)(2,1)S(1)}, bf16[768,64]{0,1:T(8,128)(2,1)}, u32[]{:S(2)}) copy-start(bf16[768,64]{0,1:T(8,128)(2,1)} %param.17) | copy-start | bytes 294916
  180.1 20.9 %copy-start.9 = (bf16[768,64]{0,1:T(8,128)(2,1)S(1)}, bf16[768,64]{0,1:T(8,128)(2,1)}, u32[]{:S(2)}) copy-start(bf16[768,64]{0,1:T(8,128)(2,1)} %param.16) | copy-start | bytes 294916
  180.1 21.0 %copy-start.1 = (bf16[1024,128]{1,0:T(8,128)(2,1)S(1)}, bf16[1024,128]{1,0:T(8,128)(2,1)}, u32[]{:S(2)}) copy-start(bf16[1024,128]{1,0:T(8,128)(2,1)} %w_ref.1) | copy-start | bytes 786436
  180.1 21.0 %copy-start.2 = (bf16[768,64]{0,1:T(8,128)(2,1)S(1)}, bf16[768,64]{0,1:T(8,128)(2,1)}, u32[]{:S(2)}) copy-start(bf16[768,64]{0,1:T(8,128)(2,1)} %param.15) | copy-start | bytes 294916
  180.2 21.0 %copy-start.3 = (f32[1,24576]{1,0:T(1,128)S(1)}, f32[1,24576]{1,0:T(1,128)}, u32[]{:S(2)}) copy-start(f32[1,24576]{1,0:T(1,128)} %cg_ref.1) | copy-start | bytes 294916
  180.2 113.0 %copy-start.6 = (bf16[2048,32]{0,1:T(8,128)(2,1)S(1)}, bf16[2048,32]{0,1:T(8,128)(2,1)}, u32[]{:S(2)}) copy-start(bf16[2048,32]{0,1:T(8,128)(2,1)} %param.27) | copy-start | bytes 393220
  180.2 113.4 %copy-start.7 = (bf16[2048,32]{0,1:T(8,128)(2,1)S(1)}, bf16[2048,32]{0,1:T(8,128)(2,1)}, u32[]{:S(2)}) copy-start(bf16[2048,32]{0,1:T(8,128)(2,1)} %param.28) | copy-start | bytes 393220
  187.2 132.4 %copy-start.5 = (bf16[512,128]{1,0:T(8,128)(2,1)S(1)}, bf16[512,128]{1,0:T(8,128)(2,1)}, u32[]{:S(2)}) copy-start(bf16[512,128]{1,0:T(8,128)(2,1)} %param.29) | copy-start | bytes 393220
  188.1 128.9 %all-to-all-start.2 = ((bf16[32,4,9,128]{3,1,2,0:T(4,128)(2,1)}), bf16[32,4,9,128]{3,1,2,0:T(4,128)(2,1)S(1)}, u32[]{:S(2)}, u32[]{:S(2)}) async-start(bf16[32,4,9,128]{3,1,2,0:T(4,128)(2,1)} %copy.40), calls=%async_computation.2 | async-start | bytes 589824 | tf_op jit(solution)/shard_map/all_to_all | solution.py:388
Sparse Core Ops, SparseCore 0:
  59.5 65.6 all-gather.1

commit v2 on v1

v2 whole, which is shorter than its diff:
```python
import functools
import jax
import jax.numpy as jnp
from jax import lax
from jax.experimental import pallas as pl
from jax.experimental.pallas import tpu as pltpu
from jax.sharding import PartitionSpec as P

HEAD = 64
TOP = 3
LOG2E = 1.4426950408889634
MESH = pl.DeviceIdType.MESH
STOPS = (2, 7, 12, 15)
neg_fill = -1e30
norm_eps = 1e-06


def in_three(value):
    hi = value.astype(jnp.bfloat16)
    left = value - hi.astype(jnp.float32)
    mid = left.astype(jnp.bfloat16)
    low = (left - mid.astype(jnp.float32)).astype(jnp.bfloat16)
    return hi, mid, low


def step_kernel(dims, stops, *refs):
    qT_ref, kv_ref, cg_ref, w_ref = refs[0:4]
    expert_ins = refs[4:15]
    out_ref, moe_ref = refs[15:17]
    kv, qs, acc, mx, hg, wb, ring_send, ring_recv, pair_send, pair_recv, head_send, head_recv = refs[17:29]
    expert_scratch_refs = refs[29:]
    Z, Y, X, R, CH = dims
    NCH = R // CH
    QT = R // 256
    NU, ND = Z // 2, Z // 2 - 1
    ep = lax.axis_index("ep")
    tp = lax.axis_index("tp")
    z, core = ep // 2, ep % 2
    y, x = tp // X, tp % X
    up = (lax.rem(ep + 2, 2 * Z), tp)
    down = (lax.rem(ep + 2 * Z - 2, 2 * Z), tp)
    partner = (2 * z + 1 - core, tp)

    def x_peer(k):
        return (ep, y * X + lax.rem(x + k, X))

    def y_peer(k):
        return (ep, lax.rem(y + k, Y) * X + x)

    barrier = pltpu.get_barrier_semaphore()
    peers = [x_peer(k) for k in range(1, X)] + [y_peer(k) for k in range(1, Y)]
    for peer in peers:
        pl.semaphore_signal(barrier, inc=1, device_id=peer, device_id_type=MESH)

    def greet(k, carry):
        pl.semaphore_signal(barrier, inc=1, device_id=(lax.rem(ep + k, 2 * Z), tp), device_id_type=MESH)
        return carry

    lax.fori_loop(1, 2 * Z, greet, 0)
    pl.semaphore_wait(barrier, len(peers) + 2 * Z - 1)

    def copy(src, dst, ssem, rsem, dev):
        return pltpu.make_async_remote_copy(
            src_ref=src, dst_ref=dst, send_sem=ssem, recv_sem=rsem,
            device_id=dev, device_id_type=MESH)

    def first(c, slot, dev):
        return copy(kv_ref.at[:, pl.ds(c * CH, CH)], kv.at[slot, c, 0],
                    ring_send.at[slot, c], ring_recv.at[slot, c], dev)

    def first_pair(c):
        return copy(kv_ref.at[:, pl.ds(c * CH, CH)], kv.at[0, c, 1],
                    pair_send.at[0, c], pair_recv.at[0, c], partner)

    def onward(slot, c, dev):
        return copy(kv.at[slot, c, 0], kv.at[slot + 1, c, 0],
                    ring_send.at[slot + 1, c], ring_recv.at[slot + 1, c], dev)

    def to_pair(slot, c):
        return copy(kv.at[slot, c, 0], kv.at[slot, c, 1],
                    pair_send.at[slot, c], pair_recv.at[slot, c], partner)

    (send_weights, dispatch, shared_first, shared_second, gather_rows, first_products,
     second_products, combine, finish, drain_experts) = expert_stages(
        (2 * Z, Y, X, expert_ins[0].shape[0]), copy, x_peer, y_peer, expert_ins, moe_ref, expert_scratch_refs)

    for c in range(NCH):
        @pl.when(z < Z - 1)
        def _():
            first(c, 1, up).start()

        @pl.when(z < ND)
        def _():
            first(c, NU + 1, down).start()

        first_pair(c).start()

    send_weights()
    dispatch()
    q_all = jnp.transpose(qT_ref[...].astype(jnp.float32)) * (HEAD ** -0.5 * LOG2E)
    q_hi, q_mid, q_lo = in_three(q_all)
    q_one = jnp.where(lax.broadcasted_iota(jnp.int32, (R, HEAD), 1) < 3, 1.0, 0.0).astype(jnp.bfloat16)
    qs[:, 0:128] = jnp.concatenate([q_hi, q_mid], axis=1)
    qs[:, 128:256] = jnp.concatenate([q_lo, q_one], axis=1)
    mx[...] = jnp.full(mx.shape, neg_fill, jnp.float32)
    acc[...] = jnp.zeros(acc.shape, jnp.float32)
    wb[...] = jnp.zeros(wb.shape, jnp.bfloat16)

    def place(h, _):
        part = w_ref[pl.ds(pl.multiple_of(h * HEAD, HEAD), HEAD), :]
        wb[pl.ds(pl.multiple_of(h * 128, 128), HEAD), 0:128] = part
        wb[pl.ds(pl.multiple_of(h * 128 + HEAD, HEAD), HEAD), 128:256] = part
        return 0

    lax.fori_loop(0, w_ref.shape[0] // HEAD, place, 0)

    shared_first()
    first_row = pl.multiple_of(ep * R, 128)
    base_gate = cg_ref[:, pl.ds(first_row, 128)][:, 0:1]

    def gate_of(block, c):
        at = pl.multiple_of(block * R + c * CH, 128)
        return (base_gate - cg_ref[:, pl.ds(at, CH)]) * LOG2E

    def score_side(pair, gate):
        hi, mid, lo = in_three(gate)
        row = lax.broadcasted_iota(jnp.int32, (HEAD, CH), 0)
        hi, mid, lo = (piece.astype(jnp.float32) for piece in (hi, mid, lo))
        gates = jnp.where(row == 0, hi, jnp.where(row == 1, mid, jnp.where(row == 2, lo, 0.0)))
        keys = pair[0:HEAD, :]
        return jnp.concatenate([keys, keys, keys, gates.astype(jnp.bfloat16)], axis=0)

    def value_side(pair):
        return jnp.concatenate([jnp.ones((HEAD, CH), jnp.bfloat16), pair[HEAD:2 * HEAD, :]], axis=0)

    def update(i, sides, masked=False):
        rows = slice(i * 256, (i + 1) * 256)
        q = qs[rows, :]
        logits = [jnp.dot(q, keys, preferred_element_type=jnp.float32) for keys, _ in sides]
        if masked:
            qi = lax.broadcasted_iota(jnp.int32, logits[0].shape, 0)
            ki = lax.broadcasted_iota(jnp.int32, logits[0].shape, 1)
            logits[0] = jnp.where(ki <= qi, logits[0], neg_fill)
        tops = [s[:, at:at + 128] for s in logits for at in range(0, CH, 128)]
        top = tops[0]
        for s in tops[1:]:
            top = jnp.maximum(top, s)
        old = mx[rows, :]
        new = jnp.maximum(old, jnp.max(top, axis=1, keepdims=True))
        wide = jnp.concatenate([new] * (CH // 128), axis=1)
        total = acc[rows, :] * jnp.exp2(old - new)
        for s, (_, values) in zip(logits, sides):
            p = jnp.exp2(s - wide).astype(jnp.bfloat16)
            total = total + lax.dot_general(
                p, values, (((1,), (1,)), ((), ())), preferred_element_type=jnp.float32)
        acc[rows, :] = total
        mx[rows, :] = new

    def sides_of(pair, block, c):
        return score_side(pair, gate_of(block, c)), value_side(pair)

    for c in range(NCH):
        side = sides_of(kv_ref[:, c * CH:(c + 1) * CH], ep, c)
        for i in range(c, QT):
            update(i, [side], i == c)

    for c in range(NCH):
        to = first_pair(c)
        to.wait_recv()

    @pl.when(core == 1)
    def _():
        for c in range(NCH):
            side = sides_of(kv[0, c, 1], ep - 1, c)
            for i in range(QT):
                update(i, [side])

    def issue(s, c):
        @pl.when(s <= z)
        def _():
            onward(s - 1, c, up).wait_recv()
            to_pair(s, c).start()

            @pl.when(jnp.logical_and(s < NU, z < Z - 1))
            def _():
                onward(s, c, up).start()

        @pl.when(jnp.logical_and(s <= ND, lax.rem(z + s, Z) < ND))
        def _():
            onward(NU + s - 1, c, down).wait_recv()

            @pl.when(s < ND)
            def _():
                onward(NU + s, c, down).start()

            @pl.when(z + s >= Z)
            def _():
                to_pair(NU + s, c).start()

    def attend(slot, c, chip):
        sides = [sides_of(kv[slot, c, 0], 2 * chip + core, c), sides_of(kv[slot, c, 1], 2 * chip + 1 - core, c)]
        for i in range(QT):
            update(i, sides)

    def consume(s, c):
        @pl.when(s <= z)
        def _():
            to_pair(s, c).wait_recv()
            attend(s, c, z - s)

        @pl.when(jnp.logical_and(s <= ND, z + s >= Z))
        def _():
            to_pair(NU + s, c).wait_recv()
            attend(NU + s, c, z + s - Z)

    steps = NU * NCH

    def step(t, _):
        @pl.when(t < steps)
        def _():
            issue(t // NCH + 1, t % NCH)

        for at, stage in zip(stops, (shared_second, gather_rows, first_products, second_products)):
            @pl.when(t == at)
            def _():
                stage()

        @pl.when(t >= 1)
        def _():
            consume((t - 1) // NCH + 1, (t - 1) % NCH)

        return 0

    lax.fori_loop(0, steps + 1, step, 0)

    quarter, half = R // 4, R // 2
    low = lax.broadcasted_iota(jnp.int32, (quarter, 128), 1) < HEAD

    def finished(at):
        a = acc[at:at + quarter, :]
        return a / pltpu.roll(a, HEAD, 1)

    for h in range(2):
        first_half = pltpu.roll(finished(h * quarter), HEAD, 1)
        second_half = finished(half + h * quarter)
        hg[h, y, x] = jnp.where(low, first_half, second_half).astype(jnp.bfloat16)

    def spread(h, phase, k):
        along_x = (h == 0) == (phase == 0)
        dev = x_peer(k) if along_x else y_peer(k)
        if phase == 0:
            ref = hg.at[h, y, x]
        elif along_x:
            ref = hg.at[h, :, x]
        else:
            ref = hg.at[h, y]
        return copy(ref, ref, head_send.at[h, phase, k], head_recv.at[h, phase, k], dev)

    def spread_in(h, phase, k):
        along_x = (h == 0) == (phase == 0)
        n = X if along_x else Y
        src_x = lax.rem(x + X - k, X)
        src_y = lax.rem(y + Y - k, Y)
        if phase == 0:
            ref = hg.at[h, y, src_x] if along_x else hg.at[h, src_y, x]
        elif along_x:
            ref = hg.at[h, :, src_x]
        else:
            ref = hg.at[h, src_y]
        return copy(ref, ref, head_send.at[h, phase, k], head_recv.at[h, phase, k], partner)

    def count(h, phase):
        return X if (h == 0) == (phase == 0) else Y

    for phase in range(2):
        for h in range(2):
            if phase == 1:
                for k in range(1, count(h, 0)):
                    spread_in(h, 0, k).wait_recv()
            for k in range(1, count(h, phase)):
                spread(h, phase, k).start()
        if phase == 0:
            combine()
        else:
            finish()

    for h in range(2):
        for k in range(1, count(h, 1)):
            spread_in(h, 1, k).wait_recv()
        heads = X * Y
        flat = hg.at[h]
        total = jnp.zeros((quarter, 256), jnp.float32)
        for pair in range(heads // 2):
            a, b = 2 * pair, 2 * pair + 1
            lhs = jnp.concatenate([flat[a // X, a % X], flat[b // X, b % X]], axis=1)
            total = total + jnp.dot(lhs, wb[pair * 256:(pair + 1) * 256, :],
                                    preferred_element_type=jnp.float32)
        out_ref[h * quarter:(h + 1) * quarter, :] = total[:, 0:128].astype(jnp.bfloat16)
        out_ref[half + h * quarter:half + (h + 1) * quarter, :] = total[:, 128:256].astype(jnp.bfloat16)

    for c in range(NCH):
        @pl.when(z < Z - 1)
        def _():
            first(c, 1, up).wait_send()

        @pl.when(z < ND)
        def _():
            first(c, NU + 1, down).wait_send()

        first_pair(c).wait_send()

    def drain(s, _):
        for c in range(NCH):
            @pl.when(s <= z)
            def _():
                to_pair(s, c).wait_send()

                @pl.when(jnp.logical_and(s < NU, z < Z - 1))
                def _():
                    onward(s, c, up).wait_send()

            @pl.when(jnp.logical_and(s <= ND, lax.rem(z + s, Z) < ND))
            def _():
                @pl.when(s < ND)
                def _():
                    onward(NU + s, c, down).wait_send()

                @pl.when(z + s >= Z)
                def _():
                    to_pair(NU + s, c).wait_send()
        return 0

    lax.fori_loop(1, NU + 1, drain, 0)
    drain_experts()
    for phase in range(2):
        for h in range(2):
            for k in range(1, count(h, phase)):
                spread(h, phase, k).wait_send()


def dot_nn(a, b):
    return jnp.dot(a, b, preferred_element_type=jnp.float32)


def dot_nt(a, b):
    return lax.dot_general(a, b, (((1,), (1,)), ((), ())), preferred_element_type=jnp.float32)


def dot_tn(a, b):
    return lax.dot_general(a, b, (((0,), (0,)), ((), ())), preferred_element_type=jnp.float32)


def iota(shape, dim):
    return lax.broadcasted_iota(jnp.int32, shape, dim)


def as_bf16(flags):
    return jnp.where(flags, 1.0, 0.0).astype(jnp.bfloat16)


def expert_stages(dims, copy, x_peer, y_peer, ins, out_ref, scratch):
    n_ep, Y, X, T = dims
    x_in, gain_in, routes_in, routes_t_in, share_in, gate_in, up_in, down_in, sgate_in, sup_in, sdown_in = ins
    (normed, ob, rb, fa, gw, uw, dw, ha, ro, cb, ps, pr, sh,
     z_sems, w_sems, y_sems, p_sems, s_sems) = scratch
    ep = lax.axis_index("ep")
    tp = lax.axis_index("tp")
    y, x = tp // X, tp % X
    D = normed.shape[1]
    DY = D // Y
    B8 = 8 * n_ep
    HU = gate_in.shape[1]

    def ep_peer(k):
        return (lax.rem(ep + k, n_ep), tp)

    def ep_from(k):
        return lax.rem(ep + n_ep - k, n_ep)

    def x_to(k):
        return lax.rem(x + k, X)

    def x_from(k):
        return lax.rem(x + X - k, X)

    def y_from(k):
        return lax.rem(y + Y - k, Y)

    def weight_copies(k, incoming):
        to, place = x_to(k), (x_from(k) if incoming else x)
        rows = pl.ds(pl.multiple_of(place * HU, HU), HU)
        return [
            copy(gate_in.at[to], gw.at[rows], w_sems.at[0, 0, k], w_sems.at[1, 0, k], x_peer(k)),
            copy(up_in.at[to], uw.at[rows], w_sems.at[0, 1, k], w_sems.at[1, 1, k], x_peer(k)),
            copy(down_in.at[to], dw.at[place], w_sems.at[0, 2, k], w_sems.at[1, 2, k], x_peer(k)),
        ]

    def send_weights():
        for k in range(1, X):
            for c in weight_copies(k, False):
                c.start()
        rows = pl.ds(pl.multiple_of(x * HU, HU), HU)
        gw[rows, :] = gate_in[x]
        uw[rows, :] = up_in[x]
        dw[x] = down_in[x]

    def out_copy(k):
        to = lax.rem(ep + k, n_ep)
        return copy(ob.at[to], rb.at[ep], z_sems.at[0, 0, k], z_sems.at[0, 1, k], ep_peer(k))

    def in_copy(k):
        return copy(ob.at[ep], rb.at[ep_from(k)], z_sems.at[0, 0, k], z_sems.at[0, 1, k], ep_peer(k))

    def back_copy(k):
        to = lax.rem(ep + k, n_ep)
        return copy(ro.at[to], cb.at[ep], z_sems.at[1, 0, k], z_sems.at[1, 1, k], ep_peer(k))

    def returned_copy(k):
        return copy(ro.at[ep], cb.at[ep_from(k)], z_sems.at[1, 0, k], z_sems.at[1, 1, k], ep_peer(k))

    def each(first, last, fn):
        def body(k, carry):
            fn(k)
            return carry
        lax.fori_loop(first, last, body, 0)

    def row_copy(k):
        return copy(fa.at[y], fa.at[y], y_sems.at[0, 0, k], y_sems.at[0, 1, k], y_peer(k))

    def row_in(k):
        return copy(fa.at[y], fa.at[y_from(k)], y_sems.at[0, 0, k], y_sems.at[0, 1, k], y_peer(k))

    def hid_copy(k):
        return copy(ha.at[y], ha.at[y], y_sems.at[1, 0, k], y_sems.at[1, 1, k], y_peer(k))

    def hid_in(k):
        return copy(ha.at[y], ha.at[y_from(k)], y_sems.at[1, 0, k], y_sems.at[1, 1, k], y_peer(k))

    def part_copy(k):
        return copy(ps.at[x_to(k)], pr.at[x], p_sems.at[0, k], p_sems.at[1, k], x_peer(k))

    def part_in(k):
        return copy(ps.at[x], pr.at[x_from(k)], p_sems.at[0, k], p_sems.at[1, k], x_peer(k))

    def share_x(k):
        return copy(sh.at[y, x], sh.at[y, x], s_sems.at[0, 0, k], s_sems.at[0, 1, k], x_peer(k))

    def share_x_in(k):
        return copy(sh.at[y, x], sh.at[y, x_from(k)], s_sems.at[0, 0, k], s_sems.at[0, 1, k], x_peer(k))

    def share_y(k):
        return copy(sh.at[y], sh.at[y], s_sems.at[1, 0, k], s_sems.at[1, 1, k], y_peer(k))

    def share_y_in(k):
        return copy(sh.at[y], sh.at[y_from(k)], s_sems.at[1, 0, k], s_sems.at[1, 1, k], y_peer(k))

    def pick(wide):
        row = iota((B8, 128), 0) % 8
        total = jnp.zeros((B8, 128), jnp.float32)
        for c in range(X):
            total = total + jnp.where(row == c, wide[:, c * 128:(c + 1) * 128], 0.0)
        return total

    def to_tiles(value):
        return value.reshape(n_ep, 8, 128).astype(jnp.bfloat16)

    def from_tiles(tiles):
        return tiles.astype(jnp.float32).reshape(B8, 128).astype(jnp.bfloat16)

    def ninth(tile, c):
        chosen = as_bf16(iota((n_ep, B8), 1) == 8 * iota((n_ep, B8), 0) + c)
        return dot_nn(chosen, tile)

    def spread_rows(value):
        expand = as_bf16(iota((B8, n_ep), 0) // 8 == iota((B8, n_ep), 1))
        return dot_nn(expand, value)

    def dispatch():
        rows = x_in[...].astype(jnp.float32)
        mean = jnp.mean(rows * rows, axis=1, keepdims=True)
        normed[...] = (rows * lax.rsqrt(mean + norm_eps) * gain_in[...]).astype(jnp.bfloat16)
        named = iota((n_ep, T), 0) * X + x
        hit = named == routes_t_in[0:1, :]
        for j in range(1, TOP):
            hit = jnp.logical_or(hit, named == routes_t_in[j:j + 1, :])
        before = as_bf16(iota((T, T), 0) < iota((T, T), 1))
        rank = dot_nn(as_bf16(hit), before)
        place = spread_rows(jnp.where(hit, rank, -1.0).astype(jnp.bfloat16))
        mine = normed[:, pl.ds(pl.multiple_of(y * DY, 128), DY)]
        slot = (iota((B8, T), 0) % 8).astype(jnp.float32)
        main = dot_nn(as_bf16(place == slot), mine)
        last = pick(dot_nn(as_bf16(place == 8.0), mine))
        for c in range(X):
            ob[:, c] = to_tiles(main[:, c * 128:(c + 1) * 128])
        ob[:, X] = to_tiles(last)
        each(1, n_ep, lambda k: out_copy(k).start())
        rb[ep] = ob[ep]

    def shared_first():
        gate = dot_nt(sgate_in[...], normed[...])
        up = dot_nt(sup_in[...], normed[...])
        sh[y, x] = (gate / (1.0 + jnp.exp(-gate)) * up).astype(jnp.bfloat16)
        for k in range(1, X):
            share_x(k).start()

    def shared_second():
        for k in range(1, X):
            share_x_in(k).wait_recv()
        for k in range(1, Y):
            share_y(k).start()

    def gather_rows():
        each(1, n_ep, lambda k: in_copy(k).wait_recv())
        tile = from_tiles(rb[:, X])
        for c in range(X):
            fa[y, 0:B8, c * 128:(c + 1) * 128] = from_tiles(rb[:, c])
            fa[y, B8:B8 + n_ep, c * 128:(c + 1) * 128] = ninth(tile, c).astype(jnp.bfloat16)
        for k in range(1, Y):
            row_copy(k).start()

    def first_products():
        for k in range(1, X):
            for c in weight_copies(k, True):
                c.wait_recv()
        for k in range(1, Y):
            row_in(k).wait_recv()
        gate = jnp.zeros((B8 + n_ep, X * HU), jnp.float32)
        up = jnp.zeros((B8 + n_ep, X * HU), jnp.float32)
        for part in range(Y):
            piece = fa[part]
            gate = gate + dot_nt(piece, gw[:, part * DY:(part + 1) * DY])
            up = up + dot_nt(piece, uw[:, part * DY:(part + 1) * DY])
        ha[y] = (gate / (1.0 + jnp.exp(-gate)) * up).astype(jnp.bfloat16)
        for k in range(1, Y):
            hid_copy(k).start()

    def second_products():
        for k in range(1, Y):
            hid_in(k).wait_recv()
        hidden = jnp.concatenate([ha[part] for part in range(Y)], axis=1)
        ends = []
        for c in range(X):
            result = dot_nn(hidden, dw[c])
            ro[:, c] = to_tiles(result[0:B8])
            ends.append(result[B8:B8 + n_ep].astype(jnp.bfloat16))
        ro[:, X] = to_tiles(pick(spread_rows(jnp.concatenate(ends, axis=1))))
        each(1, n_ep, lambda k: back_copy(k).start())
        cb[ep] = ro[ep]

    def combine():
        named = iota((T, n_ep), 1) * X + x
        hit = jnp.zeros((T, n_ep), jnp.float32)
        weight = jnp.zeros((T, n_ep), jnp.float32)
        for j in range(TOP):
            same = named == routes_in[:, j:j + 1]
            hit = hit + jnp.where(same, 1.0, 0.0)
            weight = weight + jnp.where(same, share_in[:, j:j + 1], 0.0)
        before = as_bf16(iota((T, T), 1) < iota((T, T), 0))
        rank = dot_nn(before, hit.astype(jnp.bfloat16))
        rank = jnp.where(hit > 0.0, rank, -1.0)
        high = weight.astype(jnp.bfloat16)
        low = (weight - high.astype(jnp.float32)).astype(jnp.bfloat16)
        widen = as_bf16(iota((n_ep, B8), 1) // 8 == iota((n_ep, B8), 0))
        at = dot_nn(rank.astype(jnp.bfloat16), widen) == (iota((T, B8), 1) % 8).astype(jnp.float32)
        end = rank == 8.0
        each(1, n_ep, lambda k: returned_copy(k).wait_recv())
        main = jnp.concatenate([from_tiles(cb[:, c]) for c in range(X)], axis=1)
        tile = from_tiles(cb[:, X])
        last = jnp.concatenate([ninth(tile, c).astype(jnp.bfloat16) for c in range(X)], axis=1)
        total = jnp.zeros((T, DY), jnp.float32)
        for piece in (high, low):
            scaled = jnp.where(at, dot_nn(piece, widen), 0.0).astype(jnp.bfloat16)
            total = total + dot_nn(scaled, main)
            total = total + dot_nn(jnp.where(end, piece.astype(jnp.float32), 0.0).astype(jnp.bfloat16), last)
        for c in range(X):
            ps[c] = total[:, c * 128:(c + 1) * 128]
        for k in range(1, X):
            part_copy(k).start()

    def finish():
        for k in range(1, Y):
            share_y_in(k).wait_recv()
        hidden = jnp.concatenate([sh[a, b] for a in range(Y) for b in range(X)], axis=0)
        total = dot_tn(hidden, sdown_in[...])
        for k in range(1, X):
            part_in(k).wait_recv()
        total = total + ps[x]
        for k in range(1, X):
            total = total + pr[x_from(k)]
        out_ref[...] = total.astype(jnp.bfloat16)

    def drain():
        each(1, n_ep, lambda k: out_copy(k).wait_send())
        each(1, n_ep, lambda k: back_copy(k).wait_send())
        for k in range(1, X):
            for c in weight_copies(k, False):
                c.wait_send()
            share_x(k).wait_send()
            part_copy(k).wait_send()
        for k in range(1, Y):
            share_y(k).wait_send()
            row_copy(k).wait_send()
            hid_copy(k).wait_send()

    return (send_weights, dispatch, shared_first, shared_second, gather_rows, first_products,
            second_products, combine, finish, drain)


def expert_scratch(n_ep, Y, X, T, D, HU, FF):
    B8 = 8 * n_ep
    tiles = (n_ep, X + 1, 8, 128)
    bf16 = jnp.bfloat16
    return [
        pltpu.VMEM((T, D), bf16),
        pltpu.VMEM(tiles, bf16),
        pltpu.VMEM(tiles, bf16),
        pltpu.VMEM((Y, B8 + n_ep, D // Y), bf16),
        pltpu.VMEM((X * HU, D), bf16),
        pltpu.VMEM((X * HU, D), bf16),
        pltpu.VMEM((X, FF, 128), bf16),
        pltpu.VMEM((Y, B8 + n_ep, X * HU), bf16),
        pltpu.VMEM(tiles, bf16),
        pltpu.VMEM(tiles, bf16),
        pltpu.VMEM((X, T, 128), jnp.float32),
        pltpu.VMEM((X, T, 128), jnp.float32),
        pltpu.VMEM((Y, X, HU, T), bf16),
        pltpu.SemaphoreType.DMA((2, 2, n_ep)),
        pltpu.SemaphoreType.DMA((2, 3, X)),
        pltpu.SemaphoreType.DMA((2, 2, Y)),
        pltpu.SemaphoreType.DMA((2, X)),
        pltpu.SemaphoreType.DMA((2, 2, 4)),
    ]


def local(
    query_rows,
    key_rows,
    value_rows,
    cum_gate,
    out_weight,
    moe_input,
    moe_gain,
    routes,
    route_weight,
    expert_gate,
    expert_up,
    expert_down,
    shared_gate,
    shared_up,
    shared_down,
):
    n_ep, n_tp = lax.axis_size("ep"), lax.axis_size("tp")
    X = expert_gate.shape[0]
    Y = n_tp // X
    Z = n_ep // 2
    R = query_rows.shape[0]
    CH = 256
    T, D = moe_input.shape
    HU = expert_gate.shape[2]
    kv = jnp.concatenate([key_rows.T, value_rows.T], axis=0)
    vm = pl.BlockSpec(memory_space=pltpu.VMEM)
    step = pl.pallas_call(
        functools.partial(step_kernel, (Z, Y, X, R, CH), STOPS),
        out_shape=(
            jax.ShapeDtypeStruct((R, out_weight.shape[1]), jnp.bfloat16),
            jax.ShapeDtypeStruct((T, out_weight.shape[1]), jnp.bfloat16),
        ),
        in_specs=[vm] * 15,
        out_specs=(vm, vm),
        scratch_shapes=[
            pltpu.VMEM((Z, R // CH, 2, 2 * HEAD, CH), jnp.bfloat16),
            pltpu.VMEM((R, 256), jnp.bfloat16),
            pltpu.VMEM((R, 128), jnp.float32),
            pltpu.VMEM((R, 128), jnp.float32),
            pltpu.VMEM((2, Y, X, R // 4, 128), jnp.bfloat16),
            pltpu.VMEM((n_tp * 128, 256), jnp.bfloat16),
            pltpu.SemaphoreType.DMA((Z, R // CH)),
            pltpu.SemaphoreType.DMA((Z, R // CH)),
            pltpu.SemaphoreType.DMA((Z, R // CH)),
            pltpu.SemaphoreType.DMA((Z, R // CH)),
            pltpu.SemaphoreType.DMA((2, 2, 4)),
            pltpu.SemaphoreType.DMA((2, 2, 4)),
        ]
        + expert_scratch(n_ep, Y, X, T, D, HU, expert_down.shape[1]),
        compiler_params=pltpu.CompilerParams(
            collective_id=0, has_side_effects=True, vmem_limit_bytes=56 * 1024 * 1024
        ),
    )
    return step(
        query_rows.T,
        kv,
        cum_gate,
        out_weight,
        moe_input,
        moe_gain[None, :],
        routes,
        routes.T,
        route_weight,
        expert_gate.swapaxes(1, 2),
        expert_up.swapaxes(1, 2),
        expert_down,
        shared_gate.T,
        shared_up.T,
        shared_down,
    )


def solution(mesh):
    placed = (
        P("ep", "tp"),
        P("ep", "tp"),
        P("ep", "tp"),
        P("tp", None),
        P(None, "tp"),
        P("ep", None),
        P(),
        P("ep", None),
        P("ep", None),
        P("ep", None, "tp"),
        P("ep", None, "tp"),
        P("ep", None, "tp"),
        P(None, "tp"),
        P(None, "tp"),
        P(None, "tp"),
    )
    return jax.shard_map(
        local, mesh=mesh, in_specs=placed, out_specs=(P("ep", "tp"), P("ep", "tp")), check_vma=False
    )
```

time: 329 us -> 119 us (0.36)
  the two profiles are of different devices: /device:TPU:2 before, /device:TPU:448 now
where the time goes in v2:
time: 119 us
  Pallas kernels  113 us (95%)
  local copies, waits for them, and re-layouts  4.47 us (4%)
    pallas_call x1, Pallas kernels, local(): step(query_rows.T, kv, cum_gate, out_weight, moe_input, moe_gain[None, :]...  113 us
    unnamed x14, local copies, waits for them, and re-layouts  4.47 us

profile of v2, /device:TPU:448, one launch (start us, length us, event | category | flops | bytes accessed | tf_op | source)
XLA Modules:
  0.0 119.1 jit_solution(6990137808813138941)
XLA Ops:
  0.6 0.0 copy-start.4
  0.6 0.0 copy-start.3
  0.7 0.7 copy-done.4
  1.3 0.0 copy-start
  1.3 0.0 copy-start.1
  1.3 0.8 copy.18.refs_8_
  2.1 0.0 copy-done.3
  2.1 0.8 copy.17.refs_6_
  2.9 0.0 copy-done
  2.9 0.0 copy-done.1
  2.9 0.7 pad_maximum_fusion.refs_1_
  3.6 113.3 %shard_map.158 = (bf16[768,128]{1,0:T(8,128)(2,1)}, bf16[192,128]{1,0:T(8,128)(2,1)}) custom-call(bf16[64,768]{1,0:T(8,128)(2,1)} %bitcast.15, bf16[128,768]{1,0:T(8,128)(2,1)} %pad_maximum_fusion.refs_1_, f32[1,24576]{1,0:T(1,128)} %refs_2_.1, bf16[1024,128]{1,0:T(8,128)(2,1)} %refs_3_.1, bf16[192,2048]{1,0:T(8,128)(2,1)} %refs_4_.1, f32[1,2048]{1,0:T(1,128)} %bitcast.17, ...), custom_call_target="tpu_custom_call" | custom-call | tf_op jit(solution)/shard_map/pallas_call | solution.py:689
  116.8 0.0 copy-start.2
  116.8 1.6 %copy.21 = bf16[768,128]{1,0:T(8,128)(2,1)} copy(bf16[768,128]{1,0:T(8,128)(2,1)} %get-tuple-element.4) | data formatting | bytes 393216
  118.5 0.0 copy-done.2
  118.5 0.6 copy.22
Async XLA Ops:
  0.6 0.7 copy-start.4
  0.6 1.4 %copy-start.3 = (s32[192,3]{0,1:T(4,128)S(1)}, s32[192,3]{0,1:T(4,128)}, u32[]{:S(2)}) copy-start(s32[192,3]{0,1:T(4,128)} %param.22) | copy-start | bytes 6916
  1.3 1.5 %copy-start = (bf16[768,64]{0,1:T(8,128)(2,1)S(1)}, bf16[768,64]{0,1:T(8,128)(2,1)}, u32[]{:S(2)}) copy-start(bf16[768,64]{0,1:T(8,128)(2,1)} %param.17) | copy-start | bytes 294916
  1.3 1.5 %copy-start.1 = (bf16[768,64]{0,1:T(8,128)(2,1)S(1)}, bf16[768,64]{0,1:T(8,128)(2,1)}, u32[]{:S(2)}) copy-start(bf16[768,64]{0,1:T(8,128)(2,1)} %param.16) | copy-start | bytes 294916
  116.8 1.6 %copy-start.2 = (bf16[192,128]{1,0:T(8,128)(2,1)S(1)}, bf16[192,128]{1,0:T(8,128)(2,1)}, u32[]{:S(2)}) copy-start(bf16[192,128]{1,0:T(8,128)(2,1)} %get-tuple-element.5) | copy-start | bytes 147460

commit v3 on v2

--- a/solution.py
+++ b/solution.py
@@ -24,8 +24,8 @@
 
 
 def step_kernel(dims, stops, *refs):
-    qT_ref, kv_ref, cg_ref, w_ref = refs[0:4]
-    expert_ins = refs[4:15]
+    qT_ref, kT_ref, vT_ref, cg_ref, w_ref = refs[0:5]
+    expert_ins = refs[5:15]
     out_ref, moe_ref = refs[15:17]
     kv, qs, acc, mx, hg, wb, ring_send, ring_recv, pair_send, pair_recv, head_send, head_recv = refs[17:29]
     expert_scratch_refs = refs[29:]
@@ -57,20 +57,29 @@
         return carry
 
     lax.fori_loop(1, 2 * Z, greet, 0)
-    pl.semaphore_wait(barrier, len(peers) + 2 * Z - 1)
 
     def copy(src, dst, ssem, rsem, dev):
         return pltpu.make_async_remote_copy(
             src_ref=src, dst_ref=dst, send_sem=ssem, recv_sem=rsem,
             device_id=dev, device_id_type=MESH)
 
+    def halves(c, target, ssem, rsem, dev):
+        keys = copy(kT_ref.at[:, pl.ds(c * CH, CH)], target.at[0:HEAD], ssem, rsem, dev)
+        values = copy(vT_ref.at[:, pl.ds(c * CH, CH)], target.at[HEAD:2 * HEAD], ssem, rsem, dev)
+        keys.start()
+        values.start()
+
+    def start_first(c, slot, dev):
+        halves(c, kv.at[slot, c, 0], ring_send.at[slot, c], ring_recv.at[slot, c], dev)
+
+    def start_first_pair(c):
+        halves(c, kv.at[0, c, 1], pair_send.at[0, c], pair_recv.at[0, c], partner)
+
     def first(c, slot, dev):
-        return copy(kv_ref.at[:, pl.ds(c * CH, CH)], kv.at[slot, c, 0],
-                    ring_send.at[slot, c], ring_recv.at[slot, c], dev)
+        return copy(kv.at[slot, c, 0], kv.at[slot, c, 0], ring_send.at[slot, c], ring_recv.at[slot, c], dev)
 
     def first_pair(c):
-        return copy(kv_ref.at[:, pl.ds(c * CH, CH)], kv.at[0, c, 1],
-                    pair_send.at[0, c], pair_recv.at[0, c], partner)
+        return copy(kv.at[0, c, 1], kv.at[0, c, 1], pair_send.at[0, c], pair_recv.at[0, c], partner)
 
     def onward(slot, c, dev):
         return copy(kv.at[slot, c, 0], kv.at[slot + 1, c, 0],
@@ -80,23 +89,13 @@
         return copy(kv.at[slot, c, 0], kv.at[slot, c, 1],
                     pair_send.at[slot, c], pair_recv.at[slot, c], partner)
 
-    (send_weights, dispatch, shared_first, shared_second, gather_rows, first_products,
-     second_products, combine, finish, drain_experts) = expert_stages(
+    (keep_weights, send_weights, dispatch, send_rows, shared_first, send_shared, shared_second,
+     gather_rows, first_products, second_products, combine, finish, drain_experts) = expert_stages(
         (2 * Z, Y, X, expert_ins[0].shape[0]), copy, x_peer, y_peer, expert_ins, moe_ref, expert_scratch_refs)
 
-    for c in range(NCH):
-        @pl.when(z < Z - 1)
-        def _():
-            first(c, 1, up).start()
-
-        @pl.when(z < ND)
-        def _():
-            first(c, NU + 1, down).start()
-
-        first_pair(c).start()
-
-    send_weights()
     dispatch()
+    shared_first()
+    keep_weights()
     q_all = jnp.transpose(qT_ref[...].astype(jnp.float32)) * (HEAD ** -0.5 * LOG2E)
     q_hi, q_mid, q_lo = in_three(q_all)
     q_one = jnp.where(lax.broadcasted_iota(jnp.int32, (R, HEAD), 1) < 3, 1.0, 0.0).astype(jnp.bfloat16)
@@ -114,7 +113,6 @@
 
     lax.fori_loop(0, w_ref.shape[0] // HEAD, place, 0)
 
-    shared_first()
     first_row = pl.multiple_of(ep * R, 128)
     base_gate = cg_ref[:, pl.ds(first_row, 128)][:, 0:1]
 
@@ -160,13 +158,27 @@
         return score_side(pair, gate_of(block, c)), value_side(pair)
 
     for c in range(NCH):
-        side = sides_of(kv_ref[:, c * CH:(c + 1) * CH], ep, c)
+        side = sides_of(jnp.concatenate([kT_ref[:, c * CH:(c + 1) * CH], vT_ref[:, c * CH:(c + 1) * CH]], axis=0), ep, c)
         for i in range(c, QT):
             update(i, [side], i == c)
 
+    pl.semaphore_wait(barrier, len(peers) + 2 * Z - 1)
     for c in range(NCH):
-        to = first_pair(c)
-        to.wait_recv()
+        @pl.when(z < Z - 1)
+        def _():
+            start_first(c, 1, up)
+
+        @pl.when(z < ND)
+        def _():
+            start_first(c, NU + 1, down)
+
+        start_first_pair(c)
+
+    send_rows()
+    send_weights()
+    send_shared()
+    for c in range(NCH):
+        first_pair(c).wait_recv()
 
     @pl.when(core == 1)
     def _():
@@ -360,8 +372,8 @@
 
 def expert_stages(dims, copy, x_peer, y_peer, ins, out_ref, scratch):
     n_ep, Y, X, T = dims
-    x_in, gain_in, routes_in, routes_t_in, share_in, gate_in, up_in, down_in, sgate_in, sup_in, sdown_in = ins
-    (normed, ob, rb, fa, gw, uw, dw, ha, ro, cb, ps, pr, sh,
+    x_in, gain_in, routes_in, share_in, gate_in, up_in, down_in, sgate_in, sup_in, sdown_in = ins
+    (normed, ob, rb, fa, gw, uw, dw, ha, ro, cb, ps, pr, sh, mix, mix_end,
      z_sems, w_sems, y_sems, p_sems, s_sems) = scratch
     ep = lax.axis_index("ep")
     tp = lax.axis_index("tp")
@@ -395,14 +407,16 @@
             copy(down_in.at[to], dw.at[place], w_sems.at[0, 2, k], w_sems.at[1, 2, k], x_peer(k)),
         ]
 
+    def keep_weights():
+        rows = pl.ds(pl.multiple_of(x * HU, HU), HU)
+        gw[rows, :] = gate_in[x]
+        uw[rows, :] = up_in[x]
+        dw[x] = down_in[x]
+
     def send_weights():
         for k in range(1, X):
             for c in weight_copies(k, False):
                 c.start()
-        rows = pl.ds(pl.multiple_of(x * HU, HU), HU)
-        gw[rows, :] = gate_in[x]
-        uw[rows, :] = up_in[x]
-        dw[x] = down_in[x]
 
     def out_copy(k):
         to = lax.rem(ep + k, n_ep)
@@ -480,12 +494,15 @@
         mean = jnp.mean(rows * rows, axis=1, keepdims=True)
         normed[...] = (rows * lax.rsqrt(mean + norm_eps) * gain_in[...]).astype(jnp.bfloat16)
         named = iota((n_ep, T), 0) * X + x
-        hit = named == routes_t_in[0:1, :]
-        for j in range(1, TOP):
-            hit = jnp.logical_or(hit, named == routes_t_in[j:j + 1, :])
+        hit = jnp.zeros((n_ep, T), jnp.float32)
+        weight = jnp.zeros((n_ep, T), jnp.float32)
+        for j in range(TOP):
+            same = named == routes_in[j:j + 1, :]
+            hit = hit + jnp.where(same, 1.0, 0.0)
+            weight = weight + jnp.where(same, share_in[j:j + 1, :], 0.0)
         before = as_bf16(iota((T, T), 0) < iota((T, T), 1))
-        rank = dot_nn(as_bf16(hit), before)
-        place = spread_rows(jnp.where(hit, rank, -1.0).astype(jnp.bfloat16))
+        rank = jnp.where(hit > 0.0, dot_nn(hit.astype(jnp.bfloat16), before), -1.0)
+        place = spread_rows(rank.astype(jnp.bfloat16))
         mine = normed[:, pl.ds(pl.multiple_of(y * DY, 128), DY)]
         slot = (iota((B8, T), 0) % 8).astype(jnp.float32)
         main = dot_nn(as_bf16(place == slot), mine)
@@ -493,13 +510,22 @@
         for c in range(X):
             ob[:, c] = to_tiles(main[:, c * 128:(c + 1) * 128])
         ob[:, X] = to_tiles(last)
+        rb[ep] = ob[ep]
+        high = weight.astype(jnp.bfloat16)
+        low = (weight - high.astype(jnp.float32)).astype(jnp.bfloat16)
+        for n, piece in enumerate((high, low)):
+            mix[n] = jnp.where(place == slot, spread_rows(piece), 0.0).astype(jnp.bfloat16)
+            mix_end[n] = jnp.where(rank == 8.0, piece.astype(jnp.float32), 0.0).astype(jnp.bfloat16)
+
+    def send_rows():
         each(1, n_ep, lambda k: out_copy(k).start())
-        rb[ep] = ob[ep]
 
     def shared_first():
         gate = dot_nt(sgate_in[...], normed[...])
         up = dot_nt(sup_in[...], normed[...])
         sh[y, x] = (gate / (1.0 + jnp.exp(-gate)) * up).astype(jnp.bfloat16)
+
+    def send_shared():
         for k in range(1, X):
             share_x(k).start()
 
@@ -548,30 +574,13 @@
         cb[ep] = ro[ep]
 
     def combine():
-        named = iota((T, n_ep), 1) * X + x
-        hit = jnp.zeros((T, n_ep), jnp.float32)
-        weight = jnp.zeros((T, n_ep), jnp.float32)
-        for j in range(TOP):
-            same = named == routes_in[:, j:j + 1]
-            hit = hit + jnp.where(same, 1.0, 0.0)
-            weight = weight + jnp.where(same, share_in[:, j:j + 1], 0.0)
-        before = as_bf16(iota((T, T), 1) < iota((T, T), 0))
-        rank = dot_nn(before, hit.astype(jnp.bfloat16))
-        rank = jnp.where(hit > 0.0, rank, -1.0)
-        high = weight.astype(jnp.bfloat16)
-        low = (weight - high.astype(jnp.float32)).astype(jnp.bfloat16)
-        widen = as_bf16(iota((n_ep, B8), 1) // 8 == iota((n_ep, B8), 0))
-        at = dot_nn(rank.astype(jnp.bfloat16), widen) == (iota((T, B8), 1) % 8).astype(jnp.float32)
-        end = rank == 8.0
         each(1, n_ep, lambda k: returned_copy(k).wait_recv())
         main = jnp.concatenate([from_tiles(cb[:, c]) for c in range(X)], axis=1)
         tile = from_tiles(cb[:, X])
         last = jnp.concatenate([ninth(tile, c).astype(jnp.bfloat16) for c in range(X)], axis=1)
         total = jnp.zeros((T, DY), jnp.float32)
-        for piece in (high, low):
-            scaled = jnp.where(at, dot_nn(piece, widen), 0.0).astype(jnp.bfloat16)
-            total = total + dot_nn(scaled, main)
-            total = total + dot_nn(jnp.where(end, piece.astype(jnp.float32), 0.0).astype(jnp.bfloat16), last)
+        for n in range(2):
+            total = total + dot_tn(mix[n], main) + dot_tn(mix_end[n], last)
         for c in range(X):
             ps[c] = total[:, c * 128:(c + 1) * 128]
         for k in range(1, X):
@@ -602,8 +611,8 @@
             row_copy(k).wait_send()
             hid_copy(k).wait_send()
 
-    return (send_weights, dispatch, shared_first, shared_second, gather_rows, first_products,
-            second_products, combine, finish, drain)
+    return (keep_weights, send_weights, dispatch, send_rows, shared_first, send_shared, shared_second,
+            gather_rows, first_products, second_products, combine, finish, drain)
 
 
 def expert_scratch(n_ep, Y, X, T, D, HU, FF):
@@ -624,6 +633,8 @@
         pltpu.VMEM((X, T, 128), jnp.float32),
         pltpu.VMEM((X, T, 128), jnp.float32),
         pltpu.VMEM((Y, X, HU, T), bf16),
+        pltpu.VMEM((2, B8, T), bf16),
+        pltpu.VMEM((2, n_ep, T), bf16),
         pltpu.SemaphoreType.DMA((2, 2, n_ep)),
         pltpu.SemaphoreType.DMA((2, 3, X)),
         pltpu.SemaphoreType.DMA((2, 2, Y)),
@@ -657,7 +668,6 @@
     CH = 256
     T, D = moe_input.shape
     HU = expert_gate.shape[2]
-    kv = jnp.concatenate([key_rows.T, value_rows.T], axis=0)
     vm = pl.BlockSpec(memory_space=pltpu.VMEM)
     step = pl.pallas_call(
         functools.partial(step_kernel, (Z, Y, X, R, CH), STOPS),
@@ -688,14 +698,14 @@
     )
     return step(
         query_rows.T,
-        kv,
+        key_rows.T,
+        value_rows.T,
         cum_gate,
         out_weight,
         moe_input,
         moe_gain[None, :],
-        routes,
         routes.T,
-        route_weight,
+        route_weight.T,
         expert_gate.swapaxes(1, 2),
         expert_up.swapaxes(1, 2),
         expert_down,

time: 119 us -> 116 us (0.975)
  local copies, waits for them, and re-layouts: 4.47 us -> 2.25 us
    unnamed x14 -> x4, local copies, waits for them, and re-layouts: 4.47 us -> 2.25 us
where the time goes in v3:
time: 116 us
  Pallas kernels  113 us (97%)
  local copies, waits for them, and re-layouts  2.25 us (2%)
    pallas_call x1, Pallas kernels, local(): step(query_rows.T, key_rows.T, value_rows.T, cum_gate, out_weight, moe_in...  113 us

profile of v3, /device:TPU:448, one launch (start us, length us, event | category | flops | bytes accessed | tf_op | source)
XLA Modules:
  0.0 116.1 jit_solution(314706707571827488)
XLA Ops:
  0.6 113.2 %shard_map.158 = (bf16[768,128]{1,0:T(8,128)(2,1)}, bf16[192,128]{1,0:T(8,128)(2,1)}) custom-call(bf16[64,768]{1,0:T(8,128)(2,1)} %bitcast.14, bf16[64,768]{1,0:T(8,128)(2,1)} %bitcast.15, bf16[64,768]{1,0:T(8,128)(2,1)} %bitcast.16, f32[1,24576]{1,0:T(1,128)} %refs_3_.1, bf16[1024,128]{1,0:T(8,128)(2,1)} %refs_4_.1, bf16[192,2048]{1,0:T(8,128)(2,1)} %refs_5_.1, ...), custom_call_target="tpu_custom_call" | custom-call | tf_op jit(solution)/shard_map/pallas_call | solution.py:699
  113.8 0.0 copy-start
  113.8 1.6 %copy.19 = bf16[768,128]{1,0:T(8,128)(2,1)} copy(bf16[768,128]{1,0:T(8,128)(2,1)} %get-tuple-element.4) | data formatting | bytes 393216
  115.4 0.0 copy-done
  115.4 0.6 copy.20
Async XLA Ops:
  113.8 1.6 %copy-start = (bf16[192,128]{1,0:T(8,128)(2,1)S(1)}, bf16[192,128]{1,0:T(8,128)(2,1)}, u32[]{:S(2)}) copy-start(bf16[192,128]{1,0:T(8,128)(2,1)} %get-tuple-element.5) | copy-start | bytes 147460

commit v4 on v3

--- a/solution.py
+++ b/solution.py
@@ -10,7 +10,7 @@
 TOP = 3
 LOG2E = 1.4426950408889634
 MESH = pl.DeviceIdType.MESH
-STOPS = (2, 7, 12, 15)
+STOPS = (2, 4, 9, 10, 12, 15, 18)
 neg_fill = -1e30
 norm_eps = 1e-06
 
@@ -232,7 +232,10 @@
         def _():
             issue(t // NCH + 1, t % NCH)
 
-        for at, stage in zip(stops, (shared_second, gather_rows, first_products, second_products)):
+        for at, stage in zip(stops, (
+            shared_second,
+            lambda: gather_rows(0), lambda: first_products(0), lambda: gather_rows(1),
+            lambda: second_products(0), lambda: first_products(1), lambda: second_products(1))):
             @pl.when(t == at)
             def _():
                 stage()
@@ -381,6 +384,7 @@
     D = normed.shape[1]
     DY = D // Y
     B8 = 8 * n_ep
+    quart, nh, bh = n_ep // 4, n_ep // 2, 4 * n_ep
     HU = gate_in.shape[1]
 
     def ep_peer(k):
@@ -418,19 +422,28 @@
             for c in weight_copies(k, False):
                 c.start()
 
+    def place_of(k):
+        return lax.rem(k + quart, n_ep)
+
+    def group_each(g, fn):
+        if g == 0:
+            each(1, quart, fn)
+            each(n_ep - quart, n_ep, fn)
+        else:
+            each(quart, n_ep - quart, fn)
+
     def out_copy(k):
         to = lax.rem(ep + k, n_ep)
-        return copy(ob.at[to], rb.at[ep], z_sems.at[0, 0, k], z_sems.at[0, 1, k], ep_peer(k))
+        return copy(ob.at[to], rb.at[place_of(k)], z_sems.at[0, 0, k], z_sems.at[0, 1, k], ep_peer(k))
 
     def in_copy(k):
-        return copy(ob.at[ep], rb.at[ep_from(k)], z_sems.at[0, 0, k], z_sems.at[0, 1, k], ep_peer(k))
+        return copy(ob.at[ep], rb.at[place_of(k)], z_sems.at[0, 0, k], z_sems.at[0, 1, k], ep_peer(k))
 
     def back_copy(k):
-        to = lax.rem(ep + k, n_ep)
-        return copy(ro.at[to], cb.at[ep], z_sems.at[1, 0, k], z_sems.at[1, 1, k], ep_peer(k))
+        return copy(ro.at[place_of(k)], cb.at[ep], z_sems.at[1, 0, k], z_sems.at[1, 1, k], (ep_from(k), tp))
 
     def returned_copy(k):
-        return copy(ro.at[ep], cb.at[ep_from(k)], z_sems.at[1, 0, k], z_sems.at[1, 1, k], ep_peer(k))
+        return copy(ro.at[0], cb.at[lax.rem(ep + k, n_ep)], z_sems.at[1, 0, k], z_sems.at[1, 1, k], ep_peer(k))
 
     def each(first, last, fn):
         def body(k, carry):
@@ -438,17 +451,17 @@
             return carry
         lax.fori_loop(first, last, body, 0)
 
-    def row_copy(k):
-        return copy(fa.at[y], fa.at[y], y_sems.at[0, 0, k], y_sems.at[0, 1, k], y_peer(k))
-
-    def row_in(k):
-        return copy(fa.at[y], fa.at[y_from(k)], y_sems.at[0, 0, k], y_sems.at[0, 1, k], y_peer(k))
-
-    def hid_copy(k):
-        return copy(ha.at[y], ha.at[y], y_sems.at[1, 0, k], y_sems.at[1, 1, k], y_peer(k))
-
-    def hid_in(k):
-        return copy(ha.at[y], ha.at[y_from(k)], y_sems.at[1, 0, k], y_sems.at[1, 1, k], y_peer(k))
+    def row_copy(g, k):
+        return copy(fa.at[g, y], fa.at[g, y], y_sems.at[g, 0, 0, k], y_sems.at[g, 0, 1, k], y_peer(k))
+
+    def row_in(g, k):
+        return copy(fa.at[g, y], fa.at[g, y_from(k)], y_sems.at[g, 0, 0, k], y_sems.at[g, 0, 1, k], y_peer(k))
+
+    def hid_copy(g, k):
+        return copy(ha.at[g, y], ha.at[g, y], y_sems.at[g, 1, 0, k], y_sems.at[g, 1, 1, k], y_peer(k))
+
+    def hid_in(g, k):
+        return copy(ha.at[g, y], ha.at[g, y_from(k)], y_sems.at[g, 1, 0, k], y_sems.at[g, 1, 1, k], y_peer(k))
 
     def part_copy(k):
         return copy(ps.at[x_to(k)], pr.at[x], p_sems.at[0, k], p_sems.at[1, k], x_peer(k))
@@ -469,24 +482,26 @@
         return copy(sh.at[y], sh.at[y_from(k)], s_sems.at[1, 0, k], s_sems.at[1, 1, k], y_peer(k))
 
     def pick(wide):
-        row = iota((B8, 128), 0) % 8
-        total = jnp.zeros((B8, 128), jnp.float32)
+        row = iota((wide.shape[0], 128), 0) % 8
+        total = jnp.zeros((wide.shape[0], 128), jnp.float32)
         for c in range(X):
             total = total + jnp.where(row == c, wide[:, c * 128:(c + 1) * 128], 0.0)
         return total
 
     def to_tiles(value):
-        return value.reshape(n_ep, 8, 128).astype(jnp.bfloat16)
+        return value.reshape(value.shape[0] // 8, 8, 128).astype(jnp.bfloat16)
 
     def from_tiles(tiles):
-        return tiles.astype(jnp.float32).reshape(B8, 128).astype(jnp.bfloat16)
+        return tiles.astype(jnp.float32).reshape(tiles.shape[0] * 8, 128).astype(jnp.bfloat16)
 
     def ninth(tile, c):
-        chosen = as_bf16(iota((n_ep, B8), 1) == 8 * iota((n_ep, B8), 0) + c)
+        n = tile.shape[0] // 8
+        chosen = as_bf16(iota((n, 8 * n), 1) == 8 * iota((n, 8 * n), 0) + c)
         return dot_nn(chosen, tile)
 
     def spread_rows(value):
-        expand = as_bf16(iota((B8, n_ep), 0) // 8 == iota((B8, n_ep), 1))
+        n = value.shape[0]
+        expand = as_bf16(iota((8 * n, n), 0) // 8 == iota((8 * n, n), 1))
         return dot_nn(expand, value)
 
     def dispatch():
@@ -510,7 +525,7 @@
         for c in range(X):
             ob[:, c] = to_tiles(main[:, c * 128:(c + 1) * 128])
         ob[:, X] = to_tiles(last)
-        rb[ep] = ob[ep]
+        rb[quart] = ob[ep]
         high = weight.astype(jnp.bfloat16)
         low = (weight - high.astype(jnp.float32)).astype(jnp.bfloat16)
         for n, piece in enumerate((high, low)):
@@ -518,7 +533,8 @@
             mix_end[n] = jnp.where(rank == 8.0, piece.astype(jnp.float32), 0.0).astype(jnp.bfloat16)
 
     def send_rows():
-        each(1, n_ep, lambda k: out_copy(k).start())
+        for g in range(2):
+            group_each(g, lambda k: out_copy(k).start())
 
     def shared_first():
         gate = dot_nt(sgate_in[...], normed[...])
@@ -535,43 +551,47 @@
         for k in range(1, Y):
             share_y(k).start()
 
-    def gather_rows():
-        each(1, n_ep, lambda k: in_copy(k).wait_recv())
-        tile = from_tiles(rb[:, X])
+    def gather_rows(g):
+        group_each(g, lambda k: in_copy(k).wait_recv())
+        span = slice(g * nh, (g + 1) * nh)
+        tile = from_tiles(rb[span, X])
         for c in range(X):
-            fa[y, 0:B8, c * 128:(c + 1) * 128] = from_tiles(rb[:, c])
-            fa[y, B8:B8 + n_ep, c * 128:(c + 1) * 128] = ninth(tile, c).astype(jnp.bfloat16)
+            fa[g, y, 0:bh, c * 128:(c + 1) * 128] = from_tiles(rb[span, c])
+            fa[g, y, bh:bh + nh, c * 128:(c + 1) * 128] = ninth(tile, c).astype(jnp.bfloat16)
         for k in range(1, Y):
-            row_copy(k).start()
-
-    def first_products():
-        for k in range(1, X):
-            for c in weight_copies(k, True):
-                c.wait_recv()
+            row_copy(g, k).start()
+
+    def first_products(g):
+        if g == 0:
+            for k in range(1, X):
+                for c in weight_copies(k, True):
+                    c.wait_recv()
         for k in range(1, Y):
-            row_in(k).wait_recv()
-        gate = jnp.zeros((B8 + n_ep, X * HU), jnp.float32)
-        up = jnp.zeros((B8 + n_ep, X * HU), jnp.float32)
+            row_in(g, k).wait_recv()
+        gate = jnp.zeros((bh + nh, X * HU), jnp.float32)
+        up = jnp.zeros((bh + nh, X * HU), jnp.float32)
         for part in range(Y):
-            piece = fa[part]
+            piece = fa[g, part]
             gate = gate + dot_nt(piece, gw[:, part * DY:(part + 1) * DY])
             up = up + dot_nt(piece, uw[:, part * DY:(part + 1) * DY])
-        ha[y] = (gate / (1.0 + jnp.exp(-gate)) * up).astype(jnp.bfloat16)
+        ha[g, y] = (gate / (1.0 + jnp.exp(-gate)) * up).astype(jnp.bfloat16)
         for k in range(1, Y):
-            hid_copy(k).start()
-
-    def second_products():
+            hid_copy(g, k).start()
+
+    def second_products(g):
         for k in range(1, Y):
-            hid_in(k).wait_recv()
-        hidden = jnp.concatenate([ha[part] for part in range(Y)], axis=1)
+            hid_in(g, k).wait_recv()
+        hidden = jnp.concatenate([ha[g, part] for part in range(Y)], axis=1)
+        span = slice(g * nh, (g + 1) * nh)
         ends = []
         for c in range(X):
             result = dot_nn(hidden, dw[c])
-            ro[:, c] = to_tiles(result[0:B8])
-            ends.append(result[B8:B8 + n_ep].astype(jnp.bfloat16))
-        ro[:, X] = to_tiles(pick(spread_rows(jnp.concatenate(ends, axis=1))))
-        each(1, n_ep, lambda k: back_copy(k).start())
-        cb[ep] = ro[ep]
+            ro[span, c] = to_tiles(result[0:bh])
+            ends.append(result[bh:bh + nh].astype(jnp.bfloat16))
+        ro[span, X] = to_tiles(pick(spread_rows(jnp.concatenate(ends, axis=1))))
+        group_each(g, lambda k: back_copy(k).start())
+        if g == 0:
+            cb[ep] = ro[quart]
 
     def combine():
         each(1, n_ep, lambda k: returned_copy(k).wait_recv())
@@ -608,8 +628,9 @@
             part_copy(k).wait_send()
         for k in range(1, Y):
             share_y(k).wait_send()
-            row_copy(k).wait_send()
-            hid_copy(k).wait_send()
+            for g in range(2):
+                row_copy(g, k).wait_send()
+                hid_copy(g, k).wait_send()
 
     return (keep_weights, send_weights, dispatch, send_rows, shared_first, send_shared, shared_second,
             gather_rows, first_products, second_products, combine, finish, drain)
@@ -623,11 +644,11 @@
         pltpu.VMEM((T, D), bf16),
         pltpu.VMEM(tiles, bf16),
         pltpu.VMEM(tiles, bf16),
-        pltpu.VMEM((Y, B8 + n_ep, D // Y), bf16),
+        pltpu.VMEM((2, Y, (B8 + n_ep) // 2, D // Y), bf16),
         pltpu.VMEM((X * HU, D), bf16),
         pltpu.VMEM((X * HU, D), bf16),
         pltpu.VMEM((X, FF, 128), bf16),
-        pltpu.VMEM((Y, B8 + n_ep, X * HU), bf16),
+        pltpu.VMEM((2, Y, (B8 + n_ep) // 2, X * HU), bf16),
         pltpu.VMEM(tiles, bf16),
         pltpu.VMEM(tiles, bf16),
         pltpu.VMEM((X, T, 128), jnp.float32),
@@ -637,7 +658,7 @@
         pltpu.VMEM((2, n_ep, T), bf16),
         pltpu.SemaphoreType.DMA((2, 2, n_ep)),
         pltpu.SemaphoreType.DMA((2, 3, X)),
-        pltpu.SemaphoreType.DMA((2, 2, Y)),
+        pltpu.SemaphoreType.DMA((2, 2, 2, Y)),
         pltpu.SemaphoreType.DMA((2, X)),
         pltpu.SemaphoreType.DMA((2, 2, 4)),
     ]

time: 116 us -> 110 us (0.948)
  the two profiles are of different devices: /device:TPU:448 before, /device:TPU:456 now
where the time goes in v4:
time: 110 us
  Pallas kernels  107 us (97%)
  local copies, waits for them, and re-layouts  2.25 us (2%)
    pallas_call x1, Pallas kernels, local(): step(query_rows.T, key_rows.T, value_rows.T, cum_gate, out_weight, moe_in...  107 us
    unnamed x4, local copies, waits for them, and re-layouts  2.25 us

profile of v4, /device:TPU:456, one launch (start us, length us, event | category | flops | bytes accessed | tf_op | source)
XLA Modules:
  0.0 110.0 jit_solution(13959090763319410359)
XLA Ops:
  0.6 107.1 %shard_map.158 = (bf16[768,128]{1,0:T(8,128)(2,1)}, bf16[192,128]{1,0:T(8,128)(2,1)}) custom-call(bf16[64,768]{1,0:T(8,128)(2,1)} %bitcast.14, bf16[64,768]{1,0:T(8,128)(2,1)} %bitcast.15, bf16[64,768]{1,0:T(8,128)(2,1)} %bitcast.16, f32[1,24576]{1,0:T(1,128)} %refs_3_.1, bf16[1024,128]{1,0:T(8,128)(2,1)} %refs_4_.1, bf16[192,2048]{1,0:T(8,128)(2,1)} %refs_5_.1, ...), custom_call_target="tpu_custom_call" | custom-call | tf_op jit(solution)/shard_map/pallas_call | solution.py:720
  107.7 0.0 copy-start
  107.7 1.6 %copy.19 = bf16[768,128]{1,0:T(8,128)(2,1)} copy(bf16[768,128]{1,0:T(8,128)(2,1)} %get-tuple-element.4) | data formatting | bytes 393216
  109.4 0.0 copy-done
  109.4 0.6 copy.20
Async XLA Ops:
  107.7 1.6 %copy-start = (bf16[192,128]{1,0:T(8,128)(2,1)S(1)}, bf16[192,128]{1,0:T(8,128)(2,1)}, u32[]{:S(2)}) copy-start(bf16[192,128]{1,0:T(8,128)(2,1)} %get-tuple-element.5) | copy-start | bytes 147460

commit v5 on v4

--- a/solution.py
+++ b/solution.py
@@ -10,7 +10,7 @@
 TOP = 3
 LOG2E = 1.4426950408889634
 MESH = pl.DeviceIdType.MESH
-STOPS = (2, 4, 9, 10, 12, 15, 18)
+STOPS = (2, 5, 10, 11, 14, 17, 20)
 neg_fill = -1e30
 norm_eps = 1e-06
 
@@ -209,21 +209,24 @@
             def _():
                 to_pair(NU + s, c).start()
 
-    def attend(slot, c, chip):
-        sides = [sides_of(kv[slot, c, 0], 2 * chip + core, c), sides_of(kv[slot, c, 1], 2 * chip + 1 - core, c)]
-        for i in range(QT):
-            update(i, sides)
-
-    def consume(s, c):
+    def attend(slot, chip):
+        for c in range(NCH):
+            sides = [sides_of(kv[slot, c, 0], 2 * chip + core, c), sides_of(kv[slot, c, 1], 2 * chip + 1 - core, c)]
+            for i in range(QT):
+                update(i, sides)
+
+    def consume(s):
         @pl.when(s <= z)
         def _():
-            to_pair(s, c).wait_recv()
-            attend(s, c, z - s)
+            for c in range(NCH):
+                to_pair(s, c).wait_recv()
+            attend(s, z - s)
 
         @pl.when(jnp.logical_and(s <= ND, z + s >= Z))
         def _():
-            to_pair(NU + s, c).wait_recv()
-            attend(NU + s, c, z + s - Z)
+            for c in range(NCH):
+                to_pair(NU + s, c).wait_recv()
+            attend(NU + s, z + s - Z)
 
     steps = NU * NCH
 
@@ -240,9 +243,9 @@
             def _():
                 stage()
 
-        @pl.when(t >= 1)
-        def _():
-            consume((t - 1) // NCH + 1, (t - 1) % NCH)
+        @pl.when(jnp.logical_and(t >= NCH, t % NCH == 0))
+        def _():
+            consume(t // NCH)
 
         return 0
 

time: 110 us -> 112 us (1.018)
  the two profiles are of different devices: /device:TPU:456 before, /device:TPU:104 now
where the time goes in v5:
time: 112 us
  Pallas kernels  109 us (97%)
  local copies, waits for them, and re-layouts  2.25 us (2%)
    pallas_call x1, Pallas kernels, local(): step(query_rows.T, key_rows.T, value_rows.T, cum_gate, out_weight, moe_in...  109 us
    unnamed x4, local copies, waits for them, and re-layouts  2.25 us

profile of v5, /device:TPU:104, one launch (start us, length us, event | category | flops | bytes accessed | tf_op | source)
XLA Modules:
  0.0 112.0 jit_solution(6478573842654663182)
XLA Ops:
  0.6 109.0 %shard_map.158 = (bf16[768,128]{1,0:T(8,128)(2,1)}, bf16[192,128]{1,0:T(8,128)(2,1)}) custom-call(bf16[64,768]{1,0:T(8,128)(2,1)} %bitcast.14, bf16[64,768]{1,0:T(8,128)(2,1)} %bitcast.15, bf16[64,768]{1,0:T(8,128)(2,1)} %bitcast.16, f32[1,24576]{1,0:T(1,128)} %refs_3_.1, bf16[1024,128]{1,0:T(8,128)(2,1)} %refs_4_.1, bf16[192,2048]{1,0:T(8,128)(2,1)} %refs_5_.1, ...), custom_call_target="tpu_custom_call" | custom-call | tf_op jit(solution)/shard_map/pallas_call | solution.py:723
  109.7 0.0 copy-start
  109.7 1.6 %copy.19 = bf16[768,128]{1,0:T(8,128)(2,1)} copy(bf16[768,128]{1,0:T(8,128)(2,1)} %get-tuple-element.4) | data formatting | bytes 393216
  111.3 0.0 copy-done
  111.3 0.6 copy.20
Async XLA Ops:
  109.7 1.6 %copy-start = (bf16[192,128]{1,0:T(8,128)(2,1)S(1)}, bf16[192,128]{1,0:T(8,128)(2,1)}, u32[]{:S(2)}) copy-start(bf16[192,128]{1,0:T(8,128)(2,1)} %get-tuple-element.5) | copy-start | bytes 147460
